TPU v7x, 32 devices: a whole 2x2x4 slice. The times are simulated.
32 devices in a mesh: sp: 8 (over z, x), tp: 4 (over y, core).
Axes of the slice: x: 2, y: 2, z: 4, core: 2. Of those that a mesh axis runs over, the one named last changes fastest.
Arguments:
- resid: bfloat16 [4096, 2048], P(('sp', 'tp')), may hold values from -6 to 6
- recurrent_input: bfloat16 [4096, 2048], P('sp', 'tp'), may hold values from -12.2 to 12.2
- recurrent_out_gate: bfloat16 [4096, 2048], P('sp', 'tp'), may hold values from -6 to 6
- filter_weight: float32 [4, 2048], P(None, 'tp'), may hold values from -3 to 3
- recurrence_gate_matrix: bfloat16 [32, 64, 64], P('tp'), may hold values from -0.75 to 0.75
- input_gate_matrix: bfloat16 [32, 64, 64], P('tp'), may hold values from -0.75 to 0.75
- channel_decay_raw: float32 [2048], P('tp'), may hold values from 4.8 to 13.5
- token_decay_boost: float32 [4096, 2048], P('sp', 'tp'), may hold values from -0.7 to 0
- output_projection_weight: bfloat16 [2048, 2048], P('tp'), may hold values from -0.375 to 0.375
- expert_norm_gain: float32 [2048], replicated, may hold values from 0.1 to 1.9
- routes: int32 [4096, 2], P('sp'), may hold values from 0 to 7, all different within a row; in each aligned block of 128 rows (0 to 127, 128 to 255, ...) at most 48 rows name the same one
- expert_pair_weight: float32 [4096, 2], P(('sp', 'tp')), may hold values from 0.2 to 0.8
- gate_weight: bfloat16 [8, 2048, 2048], P('sp', None, 'tp'), may hold values from -0.125 to 0.125
- up_weight: bfloat16 [8, 2048, 2048], P('sp', None, 'tp'), may hold values from -0.125 to 0.125
- down_weight: bfloat16 [8, 2048, 2048], P('sp', None, 'tp'), may hold values from -0.25 to 0.25
Outputs:
- layer_out: bfloat16 [4096, 2048], P(('sp', 'tp'))
Inputs may be any that keep to these rules, and one draw needn't show every extreme that they name: `routes`: in each aligned block of 128 rows no expert is named by more than 48 rows, and the two experts of a row differ.
All inputs are finite; a program needn't handle non-finite values.
Results may differ from a plain program's by a relative error of at most 0.013.
Values may be sent and summed in bfloat16 or wider, within the bound.
No kernel may reach another device: no remote copies, remote signals or barrier semaphores. Data moves between devices by JAX's collectives and lax.ppermute only.
A program may use at most 128 MiB of HBM per device.

v0:
```python
import functools

import jax
import jax.numpy as jnp
from jax import lax
from jax.experimental import pallas as pl
from jax.experimental.pallas import tpu as pltpu
from jax.sharding import PartitionSpec as P


RECURRENT_SCALE = 8.0
EPSILON = 1e-06


def granted(mebibytes):
    return pltpu.CompilerParams(vmem_limit_bytes=mebibytes * 2**20)


def shifted(block):
    size = lax.axis_size("sp")
    return lax.ppermute(block, "sp", [(i, i + 1) for i in range(size - 1)])


def across(block, bits):
    return lax.ppermute(block, "sp", [(i, i ^ bits) for i in range(lax.axis_size("sp"))])


def swapped(block):
    return lax.ppermute(block, "tp", [(i, i ^ 1) for i in range(lax.axis_size("tp"))])


def turned(block, distance):
    size = lax.axis_size("tp")
    return lax.ppermute(block, "tp", [(i, (i + 2 * distance) % size) for i in range(size)])


LANES = 128
GROUPS = 2
SEGMENTS = 8


def block_diagonal(blocks):
    count, width, _ = blocks.shape
    empty = jnp.zeros((width, width), blocks.dtype)
    rows = []
    for i in range(count):
        rows.append(jnp.concatenate([blocks[i] if j == i else empty for j in range(count)], axis=1))
    return jnp.concatenate(rows, axis=0)


def scan_kernel(rim, x, taps, recur, inward, slope, boost, local, running, total, wide, decays, drives):
    tokens, _ = x.shape
    margin = rim.shape[0]
    count = taps.shape[0]
    wide[0:margin, :] = rim[...].astype(jnp.float32)
    wide[margin : margin + tokens, :] = x[...].astype(jnp.float32)
    first = margin - count + 1
    mixed = wide[first : first + tokens, :] * taps[0:1, :]
    for j in range(1, count):
        mixed = mixed + wide[first + j : first + j + tokens, :] * taps[j : j + 1, :]
    smoothed = mixed.astype(jnp.bfloat16)
    recur_gate = jax.nn.sigmoid(
        jnp.dot(smoothed, block_diagonal(recur), preferred_element_type=jnp.float32)
    )
    input_gate = jax.nn.sigmoid(
        jnp.dot(smoothed, block_diagonal(inward), preferred_element_type=jnp.float32)
    )
    log_decay = -RECURRENT_SCALE * recur_gate * jax.nn.softplus(-slope[...]) + boost[...]
    decay = jnp.exp(log_decay)
    twice = 2.0 * log_decay
    series = 1.0 + twice * (1.0 / 9.0)
    for n in range(8, 1, -1):
        series = 1.0 + twice * (1.0 / n) * series
    lost = jnp.where(twice > -0.35, -twice * series, 1.0 - decay * decay)
    drive = jnp.sqrt(lost) * (input_gate * smoothed.astype(jnp.float32))
    groups, width = decays.shape[0], decays.shape[2]
    for g in range(groups):
        decays[g] = decay[:, g * width : (g + 1) * width]
        drives[g] = drive[:, g * width : (g + 1) * width]
    length = tokens // SEGMENTS

    def step(j, held):
        here = pl.ds(j, SEGMENTS, stride=length)
        after = []
        for g, (product, state) in enumerate(held):
            a = decays[g, here, :]
            state = a * state + drives[g, here, :]
            product = product * a
            local[g, here, :] = state
            running[g, here, :] = product
            after.append((product, state))
        return tuple(after)

    start = (jnp.ones((SEGMENTS, width), jnp.float32), jnp.zeros((SEGMENTS, width), jnp.float32))
    ends = lax.fori_loop(0, length, step, (start,) * groups, unroll=8)
    for g, (product, state) in enumerate(ends):
        a, b = product[0:1], state[0:1]
        for k in range(1, SEGMENTS):
            a, b = a * product[k : k + 1], product[k : k + 1] * b + state[k : k + 1]
        total[0:1, g * width : (g + 1) * width] = a
        total[1:2, g * width : (g + 1) * width] = b


def local_scan(rim, x, taps, recur, inward, slope, boost):
    tokens, channels = x.shape
    groups = min(GROUPS, channels // LANES)
    lanes = groups * LANES
    width = recur.shape[1]
    folded = pl.BlockSpec((groups, tokens, LANES), lambda i: (i, 0, 0))
    column = lambda rows: pl.BlockSpec((rows, lanes), lambda i: (0, i))
    blocks = pl.BlockSpec((lanes // width, width, width), lambda i: (i, 0, 0))
    wide = jax.ShapeDtypeStruct((channels // LANES, tokens, LANES), jnp.float32)
    return pl.pallas_call(
        scan_kernel,
        grid=(channels // lanes,),
        in_specs=[
            column(rim.shape[0]),
            column(tokens),
            column(taps.shape[0]),
            blocks,
            blocks,
            column(1),
            column(tokens),
        ],
        out_specs=[folded, folded, column(2)],
        out_shape=[wide, wide, jax.ShapeDtypeStruct((2, channels), jnp.float32)],
        scratch_shapes=[
            pltpu.VMEM((tokens + rim.shape[0], lanes), jnp.float32),
            pltpu.VMEM((groups, tokens, LANES), jnp.float32),
            pltpu.VMEM((groups, tokens, LANES), jnp.float32),
        ],
        name="local_scan",
    )(rim, x, taps, recur, inward, slope, boost)


def branch_kernel(place, entering, local, running, gate, keep, give):
    groups, tokens, width = local.shape
    length = tokens // SEGMENTS
    pairs, rows = keep.shape[0], keep.shape[1]
    step = min(length, rows)
    begins = [entering[:, g * width : (g + 1) * width] for g in range(groups)]
    for start in range(0, tokens, step):
        here = slice(start, start + step)
        states = [local[g, here, :] + running[g, here, :] * begins[g] for g in range(groups)]
        opened = jax.nn.gelu(gate[here, :].astype(jnp.float32))
        value = (opened * jnp.concatenate(states, axis=1)).astype(jnp.bfloat16)
        block = start // rows
        slot = lax.rem(block // 2 - place[0] + pairs, pairs)
        inside = slice(start % rows, start % rows + step)
        mine = place[1] == block % 2

        @pl.when(mine)
        def _():
            keep[slot, inside, :] = value

        @pl.when(jnp.logical_not(mine))
        def _():
            give[slot, inside, :] = value

        if (start + step) % length == 0:
            begins = [state[step - 1 : step] for state in states]


def finish_branch(place, entering, local, running, gate, pairs):
    tokens, channels = gate.shape
    groups = min(GROUPS, channels // LANES)
    lanes = groups * LANES
    column = lambda rows: pl.BlockSpec((rows, lanes), lambda i: (0, i))
    folded = pl.BlockSpec((groups, tokens, LANES), lambda i: (i, 0, 0))
    rows = tokens // (2 * pairs)
    half = jax.ShapeDtypeStruct((pairs, rows, channels), jnp.bfloat16)
    return pl.pallas_call(
        branch_kernel,
        grid=(channels // lanes,),
        in_specs=[
            pl.BlockSpec(memory_space=pltpu.SMEM),
            column(1),
            folded,
            folded,
            column(tokens),
        ],
        out_specs=[pl.BlockSpec((pairs, rows, lanes), lambda i: (0, 0, i))] * 2,
        out_shape=[half, half],
        cost_estimate=pl.CostEstimate(
            flops=20 * tokens * channels, bytes_accessed=12 * tokens * channels, transcendentals=0
        ),
        name="finish_branch",
    )(place, entering, local, running, gate)


def padded(count):
    return -(-count // 16) * 16


def send_kernel(resid, own, gain, slots, *refs, experts):
    pieces, (stream, *blocks) = refs[: -1 - experts], refs[-1 - experts :]
    total = own[...]
    for piece in pieces:
        total = total + piece[...].astype(jnp.float32)
    rounded = (resid[...].astype(jnp.float32) + total).astype(jnp.bfloat16)
    stream[...] = rounded
    wide = rounded.astype(jnp.float32)
    scale = lax.rsqrt(jnp.mean(wide * wide, axis=1, keepdims=True) + EPSILON)
    normed = (wide * scale * gain[...]).astype(jnp.bfloat16)
    rows = resid.shape[0]
    stride = padded(blocks[0].shape[0])
    numbers = lax.broadcasted_iota(jnp.int32, (len(blocks) * stride, rows), 0)
    hit = (numbers == slots[0:1, :]) | (numbers == slots[1:2, :])
    picked = jnp.dot(
        hit.astype(jnp.float32).astype(jnp.bfloat16), normed, preferred_element_type=jnp.float32
    ).astype(jnp.bfloat16)
    for i, block in enumerate(blocks):
        block[...] = picked[i * stride : i * stride + block.shape[0]]


def send_rows(resid, own, pieces, gain, slots, experts, capacity):
    rows, width = resid.shape
    block = jax.ShapeDtypeStruct((capacity, width), jnp.bfloat16)
    stream, *blocks = pl.pallas_call(
        functools.partial(send_kernel, experts=experts),
        out_shape=[jax.ShapeDtypeStruct((rows, width), jnp.bfloat16)] + [block] * experts,
        cost_estimate=pl.CostEstimate(
            flops=2 * rows * width * experts * capacity,
            bytes_accessed=8 * rows * width,
            transcendentals=0,
        ),
        compiler_params=granted(14),
        name="send_rows",
    )(resid, own, gain, slots, *pieces)
    return stream, blocks


def expert_kernel(place, *refs, groups, outs, pairs):
    rows_in, refs = refs[:groups], refs[groups:]
    (gate_own, up_own, gate_far, up_far, *downs), refs = refs[: 4 + 2 * pairs], refs[4 + 2 * pairs :]
    rows_out, (left, active) = refs[:outs], refs[outs:]
    hidden = gate_own.shape[1]
    strip, width = 2 * hidden, downs[0].shape[1]
    at = 0
    for block in rows_in:
        left[at : at + block.shape[0], :] = block[...]
        at += block.shape[0]
    step = min(256, hidden)
    for side, (gates, ups) in enumerate(((gate_own, up_own), (gate_far, up_far))):
        core = place[1] if side == 0 else 1 - place[1]
        for start in range(0, hidden, step):
            here = slice(start, start + step)
            gate = jnp.dot(left[...], gates[:, here], preferred_element_type=jnp.float32)
            upward = jnp.dot(left[...], ups[:, here], preferred_element_type=jnp.float32)
            there = pl.ds(pl.multiple_of(core * hidden + start, step), step)
            active[:, there] = (jax.nn.silu(gate) * upward).astype(jnp.bfloat16)
    for i, down in enumerate(downs):
        if i < 2:
            side, d = i, 0
            piece = down[pl.ds(pl.multiple_of(place[0] * strip, strip), strip), :]
        else:
            side, d = (i - 2) // (pairs - 1), (i - 2) % (pairs - 1) + 1
            piece = down[...]
        core = place[1] if side == 0 else 1 - place[1]
        column = (lax.rem(place[0] - d + pairs, pairs) * 2 + core) * width
        there = pl.ds(pl.multiple_of(column, width), width)
        result = jnp.dot(active[...], piece, preferred_element_type=jnp.float32)
        at = 0
        for block in rows_out:
            block[:, there] = result[at : at + block.shape[0]].astype(block.dtype)
            at += block.shape[0]


def expert_rows(place, rows, outs, weights):
    *gates, downs = weights
    model, hidden = gates[0].shape
    pairs = len(downs) // 2
    height = sum(a.shape[0] for a in rows)
    vmem = pl.BlockSpec(memory_space=pltpu.VMEM)
    return pl.pallas_call(
        functools.partial(expert_kernel, groups=len(rows), outs=len(outs), pairs=pairs),
        in_specs=[pl.BlockSpec(memory_space=pltpu.SMEM)]
        + [vmem] * (len(rows) + 4 + 2 * pairs),
        out_specs=[vmem] * len(outs),
        out_shape=[jax.ShapeDtypeStruct((count, model), kind) for count, kind in outs],
        scratch_shapes=[
            pltpu.VMEM((height, model), jnp.bfloat16),
            pltpu.VMEM((height, 2 * hidden), jnp.bfloat16),
        ],
        cost_estimate=pl.CostEstimate(
            flops=12 * height * model * hidden,
            bytes_accessed=12 * model * hidden,
            transcendentals=0,
        ),
        compiler_params=granted(28),
        name="expert_rows",
    )(place, *rows, *gates, *downs)


def mix_kernel(slots, pair_weight, mix):
    rows = slots.shape[0]
    numbers = lax.broadcasted_iota(jnp.int32, (rows, mix.shape[1]), 1)
    share = jnp.where(numbers == slots[:, 0:1], pair_weight[:, 0:1], 0.0)
    share = share + jnp.where(numbers == slots[:, 1:2], pair_weight[:, 1:2], 0.0)
    high = share.astype(jnp.bfloat16)
    mix[0:rows, :] = high
    mix[rows : 2 * rows, :] = (share - high.astype(jnp.float32)).astype(jnp.bfloat16)


def mix_weights(slots, pair_weight, count):
    return pl.pallas_call(
        mix_kernel,
        out_shape=jax.ShapeDtypeStruct((2 * slots.shape[0], count), jnp.bfloat16),
        compiler_params=granted(4),
        name="mix_weights",
    )(slots, pair_weight)


def blend_kernel(stream, mix, *refs):
    blocks, (out, table) = refs[:-2], refs[-2:]
    rows = stream.shape[0]
    stride = padded(blocks[0].shape[0])
    if stride != blocks[0].shape[0]:
        table[...] = jnp.zeros(table.shape, table.dtype)
    for i, block in enumerate(blocks):
        table[i * stride : i * stride + block.shape[0], :] = block[...]
    halves = jnp.dot(mix[...], table[...], preferred_element_type=jnp.float32)
    blended = halves[0:rows] + halves[rows:]
    out[...] = (stream[...].astype(jnp.float32) + blended).astype(jnp.bfloat16)


def blend_rows(stream, mix, blocks):
    rows, width = stream.shape
    lanes = min(1024, width)
    column = lambda count: pl.BlockSpec((count, lanes), lambda i: (0, i))
    fixed = lambda a: pl.BlockSpec(a.shape, lambda i: (0, 0))
    height = len(blocks) * padded(blocks[0].shape[0])
    return pl.pallas_call(
        blend_kernel,
        grid=(width // lanes,),
        in_specs=[column(rows), fixed(mix)] + [column(b.shape[0]) for b in blocks],
        out_specs=column(rows),
        out_shape=jax.ShapeDtypeStruct((rows, width), jnp.bfloat16),
        scratch_shapes=[pltpu.VMEM((height, lanes), jnp.bfloat16)],
        cost_estimate=pl.CostEstimate(
            flops=4 * rows * width * height, bytes_accessed=10 * rows * width, transcendentals=0
        ),
        compiler_params=granted(14),
        name="blend_rows",
    )(stream, mix, *blocks)


def slot_numbers(picks, experts):
    flat = picks.reshape(-1)
    onehot = (flat[:, None] == jnp.arange(experts, dtype=jnp.int32)[None, :]).astype(jnp.int32)
    before = jnp.cumsum(onehot, axis=0) - onehot
    return (flat, jnp.sum(before * onehot, axis=1))


def entering_state(total, me):
    size = lax.axis_size("sp")
    a, b = total[0:1], total[1:2]
    before = jnp.zeros_like(b)
    passed = jnp.ones_like(a)
    bit = 1
    while bit < size:
        other = across(jnp.concatenate([a, b], axis=0), bit)
        oa, ob = other[0:1], other[1:2]
        after = (me & bit) != 0
        before = jnp.where(after, passed * ob + before, before)
        passed = jnp.where(after, passed * oa, passed)
        b = jnp.where(after, a * ob + b, oa * b + ob)
        a = a * oa
        bit *= 2
    return before


def body(
    resid,
    recurrent_input,
    recurrent_out_gate,
    filter_weight,
    recurrence_gate_matrix,
    input_gate_matrix,
    channel_decay_raw,
    token_decay_boost,
    output_projection_weight,
    expert_norm_gain,
    routes,
    expert_pair_weight,
    gate_weight,
    up_weight,
    down_weight,
):
    tokens_here = recurrent_input.shape[0]
    tp_size, experts = lax.axis_size("tp"), lax.axis_size("sp")
    me, column = lax.axis_index("sp"), lax.axis_index("tp")
    pairs = tp_size // 2
    row, core = column // 2, column % 2
    place = jnp.stack([row, core]).astype(jnp.int32)
    rows_dev = tokens_here // tp_size
    capacity = max(2, 3 * rows_dev // experts)

    gate_own, up_own, down_all = gate_weight[0], up_weight[0], down_weight[0]
    strip = down_all.shape[0] // pairs
    strip_of = lambda d: lax.dynamic_slice_in_dim(down_all, lax.rem(row + d, pairs) * strip, strip, 0)
    rim = shifted(recurrent_input[tokens_here - 8 :])
    down_own = [turned(strip_of(d), d) for d in range(1, pairs)]
    projection_far = swapped(output_projection_weight)
    gate_far, up_far = swapped(gate_own), swapped(up_own)
    down_far = [swapped(piece) for piece in down_own]
    down_whole = [down_all, swapped(down_all)]
    weights = (gate_own, up_own, gate_far, up_far, down_whole + down_own + down_far)

    local, running, total = local_scan(
        rim,
        recurrent_input,
        filter_weight,
        recurrence_gate_matrix,
        input_gate_matrix,
        channel_decay_raw[None, :],
        token_decay_boost,
    )

    own_routes = lax.dynamic_slice_in_dim(routes, column * rows_dev, rows_dev, 0)
    own_flat, own_rank = slot_numbers(own_routes, experts)
    slots = ((own_flat ^ me) * padded(capacity) + own_rank).reshape(rows_dev, 2)

    before = entering_state(total, me)
    keep, give = finish_branch(place, before, local, running, recurrent_out_gate, pairs)
    taken = swapped(give)

    def projected(d):
        near = jnp.dot(keep[d], output_projection_weight, preferred_element_type=jnp.float32)
        return near + jnp.dot(taken[d], projection_far, preferred_element_type=jnp.float32)

    pieces = [turned(projected(d).astype(jnp.bfloat16), d) for d in range(1, pairs)]
    stream, blocks = send_rows(
        resid,
        projected(0),
        pieces,
        expert_norm_gain[None, :],
        slots.T,
        experts,
        capacity,
    )
    cuts = row_cuts(experts)
    arrived = {0: blocks[0]}
    for k in range(1, experts):
        arrived[k] = across(blocks[k], k)
    own = [jnp.concatenate([arrived[k] for k in range(*cut)], axis=0) for cut in cuts]
    theirs = [[turned(g, d) for d in range(1, pairs)] for g in own]
    hops = range(1, pairs)
    splits = return_cuts(experts)

    def run(chosen):
        rows = [own[i] for i in chosen] + [g for i in chosen for g in theirs[i]]
        outs = []
        for kind, count in ((jnp.float32, 1), (jnp.bfloat16, pairs - 1)):
            for i in chosen:
                parts = [((b - a) * capacity, kind) for a, b in splits if cuts[i][0] <= a < cuts[i][1]]
                outs += parts * count
        results = iter(expert_rows(place, rows, outs, weights))
        wide = {s: next(results) for i in chosen for s in inner(i)}
        narrow = {s: [] for i in chosen for s in inner(i)}
        for i in chosen:
            for _ in hops:
                for s in inner(i):
                    narrow[s].append(next(results))
        return wide, narrow

    def inner(i):
        return [s for s in splits if cuts[i][0] <= s[0] < cuts[i][1]]

    returned = {}
    for chosen in ((0, 1), (2,), (3,)):
        wide, narrow = run(chosen)
        for cut in wide:
            sums = wide[cut]
            for d in hops:
                back = turned(narrow[cut][d - 1], pairs - d)
                sums = sums + back.astype(jnp.float32)
            for j, k in enumerate(range(*cut)):
                result = sums[j * capacity : (j + 1) * capacity].astype(jnp.bfloat16)
                returned[k] = across(result, k) if k else result
    mix = mix_weights(slots, expert_pair_weight, experts * padded(capacity))
    return blend_rows(stream, mix, [returned[k] for k in range(experts)])


def row_cuts(experts):
    quarter = experts // 4
    return [(0, 1), (1, 2 * quarter), (2 * quarter, 3 * quarter), (3 * quarter, experts)]


def return_cuts(experts):
    first, near, far, last = row_cuts(experts)
    middle = (far[0] + far[1]) // 2
    return [first, near, (far[0], middle), (middle, far[1]), last]


def solution(mesh):
    placed = (
        P(("sp", "tp"), None),
        P("sp", "tp"),
        P("sp", "tp"),
        P(None, "tp"),
        P("tp", None, None),
        P("tp", None, None),
        P("tp"),
        P("sp", "tp"),
        P("tp", None),
        P(),
        P("sp", None),
        P(("sp", "tp"), None),
        P("sp", None, "tp"),
        P("sp", None, "tp"),
        P("sp", None, "tp"),
    )

    return jax.shard_map(
        body, mesh=mesh, in_specs=placed, out_specs=P(("sp", "tp"), None), check_vma=False
    )
```

profile of v0, /device:TPU:0, one launch (start us, length us, event | category | flops | bytes accessed | tf_op | source)
XLA Modules:
  0.0 206.9 jit_solution(12203484950626033733)
XLA Ops:
  0.7 4.9 %collective-permute-start = (bf16[8,512]{1,0:T(8,128)(2,1)S(1)}, bf16[8,512]{1,0:T(8,128)(2,1)S(1)}, u32[]{:S(2)}, u32[]{:S(2)}) collective-permute-start(bf16[8,512]{1,0:T(8,128)(2,1)S(1)} %slice.63), channel_id=1, source_target_pairs={{0,4},{4,8},{8,12},{12,16},{16,20},{20,24},{24,28},{1,5},{5,9},{9,... | collective-permute-start | bytes 24584 | tf_op jit(solution)/shard_map/ppermute | solution.py:21
  5.7 2.3 %dynamic-slice_bitcast_fusion = bf16[1024,512]{1,0:T(8,128)(2,1)} fusion(bf16[1,2048,512]{2,1,0:T(8,128)(2,1)} %param.29, s32[]{:T(128)S(6)} %select_n.66), kind=kLoop, calls=%fused_computation.4 | loop fusion | bytes 2097156 | tf_op jit(solution)/shard_map/dynamic_slice | solution.py:401
  11.9 7.6 %local_scan.1 = (f32[4,512,128]{2,1,0:T(8,128)}, f32[4,512,128]{2,1,0:T(8,128)}, f32[2,512]{1,0:T(2,128)}) custom-call(bf16[8,512]{1,0:T(8,128)(2,1)} %copy-done.16, bf16[512,512]{1,0:T(8,128)(2,1)} %x.1, f32[4,512]{1,0:T(4,128)} %taps.1, bf16[8,64,64]{2,1,0:T(8,128)(2,1)} %recur.1, bf16[8,64,64]{2,1,0:T(8,128)(2,1)} %inward.1, f32[1,512]{1,0:T(1,128)} %bitcast.40, ...), custom_call_target="tpu_custom_call" | custom-call | tf_op jit(solution)/shard_map/local_scan/pallas_call | solution.py:113
  21.3 2.0 collective-permute-done.1
  27.8 2.7 %collective-permute-start.3 = (f32[2,512]{1,0:T(2,128)S(1)}, f32[2,512]{1,0:T(2,128)S(1)}, u32[]{:S(2)}, u32[]{:S(2)}) collective-permute-start(f32[2,512]{1,0:T(2,128)S(1)} %pad_maximum_fusion.1), channel_id=1, source_target_pairs={{0,16},{4,20},{8,24},{12,28},{16,0},{20,4},{24,8},{28,12},{1,17},{... | collective-permute-start | bytes 12296 | tf_op jit(solution)/shard_map/ppermute | solution.py:25
  33.0 2.7 %finish_branch.1 = (bf16[2,128,512]{2,1,0:T(8,128)(2,1)}, bf16[2,128,512]{2,1,0:T(8,128)(2,1)}) custom-call(s32[2]{0:T(128)} %pad_add_fusion.place, f32[1,512]{1,0:T(1,128)} %broadcast_select_fusion.6.entering, f32[4,512,128]{2,1,0:T(8,128)} %get-tuple-element.30.local, f32[4,512,128]{2,1,0:T(8,128)} %get-tuple-element.31.running, bf16[512,512]{1,0:T(8,128)(2,1)} %gate.1), custom_call_target="tpu_custom_call" | custom-call | flops 5242880 | bytes 3145728 | tf_op jit(solution)/shard_map/finish_branch/pallas_call | solution.py:172
  35.7 2.2 %fusion.1 = f32[128,2048]{1,0:T(8,128)S(1)} fusion(bf16[512,2048]{1,0:T(8,128)(2,1)} %param.23, bf16[2,128,512]{2,1,0:T(8,128)(2,1)} %get-tuple-element.32), kind=kOutput, calls=%fused_computation.11 | convolution fusion | flops 268435456 | bytes 3276800 | tf_op jit(solution)/shard_map/dot_general | solution.py:429
  38.5 2.3 %fusion = bf16[128,2048]{1,0:T(8,128)(2,1)S(1)} fusion(f32[128,2048]{1,0:T(8,128)S(1)} %fusion.1, bf16[512,2048]{1,0:T(8,128)(2,1)} %collective-permute-done.5, bf16[2,128,512]{2,1,0:T(8,128)(2,1)S(1)} %collective-permute-done.4), kind=kOutput, calls=%fused_computation.2 | convolution fusion | flops 268959744 | bytes 3801088 | tf_op jit(solution)/shard_map/dot_general | solution.py:430
  41.8 2.1 %convolution_add_fusion.1.own = f32[128,2048]{1,0:T(8,128)S(1)} fusion(f32[128,2048]{1,0:T(8,128)S(1)} %fusion.3, bf16[512,2048]{1,0:T(8,128)(2,1)} %collective-permute-done.5, bf16[2,128,512]{2,1,0:T(8,128)(2,1)S(1)} %collective-permute-done.4), kind=kOutput, calls=%fused_computation.1 | convolution fusion | flops 268697600 | bytes 4325376 | tf_op jit(solution)/shard_map/dot_general | solution.py:430
  44.0 10.7 %collective-permute-done.6.refs_0_ = bf16[128,2048]{1,0:T(8,128)(2,1)S(1)} collective-permute-done((bf16[128,2048]{1,0:T(8,128)(2,1)S(1)}, bf16[128,2048]{1,0:T(8,128)(2,1)S(1)}, u32[]{:S(2)}, u32[]{:S(2)}) %collective-permute-start.6) | collective-permute-done | bytes 524320 | tf_op jit(solution)/shard_map/ppermute | solution.py:34
  61.1 3.6 %collective-permute-start.29 = (bf16[48,2048]{1,0:T(8,128)(2,1)}, bf16[48,2048]{1,0:T(8,128)(2,1)}, u32[]{:S(2)}, u32[]{:S(2)}) collective-permute-start(bf16[48,2048]{1,0:T(8,128)(2,1)} %get-tuple-element.49), channel_id=1, source_target_pairs={{0,24},{4,28},{8,16},{12,20},{16,8},{20,12},{24,0},{28,4},{1,25},{... | collective-permute-start | bytes 589832 | tf_op jit(solution)/shard_map/ppermute | solution.py:25
  65.1 4.3 %collective-permute-done.29 = bf16[48,2048]{1,0:T(8,128)(2,1)} collective-permute-done((bf16[48,2048]{1,0:T(8,128)(2,1)}, bf16[48,2048]{1,0:T(8,128)(2,1)}, u32[]{:S(2)}, u32[]{:S(2)}) %collective-permute-start.29) | collective-permute-done | bytes 196640 | tf_op jit(solution)/shard_map/ppermute | solution.py:25
  69.4 4.8 %collective-permute-start.22 = (bf16[48,2048]{1,0:T(8,128)(2,1)}, bf16[48,2048]{1,0:T(8,128)(2,1)S(1)}, u32[]{:S(2)}, u32[]{:S(2)}) collective-permute-start(bf16[48,2048]{1,0:T(8,128)(2,1)} %copy-done.13), channel_id=1, source_target_pairs={{0,16},{4,20},{8,24},{12,28},{16,0},{20,4},{24,8},{28,12},{1,17},{... | collective-permute-start | bytes 589832 | tf_op jit(solution)/shard_map/ppermute | solution.py:25
  75.1 6.9 %collective-permute-done.22 = bf16[48,2048]{1,0:T(8,128)(2,1)S(1)} collective-permute-done((bf16[48,2048]{1,0:T(8,128)(2,1)}, bf16[48,2048]{1,0:T(8,128)(2,1)S(1)}, u32[]{:S(2)}, u32[]{:S(2)}) %collective-permute-start.22) | collective-permute-done | bytes 196640 | tf_op jit(solution)/shard_map/ppermute | solution.py:25
  82.0 2.9 %collective-permute-start.7 = (bf16[48,2048]{1,0:T(8,128)(2,1)}, bf16[48,2048]{1,0:T(8,128)(2,1)S(1)}, u32[]{:S(2)}, u32[]{:S(2)}) collective-permute-start(bf16[48,2048]{1,0:T(8,128)(2,1)} %copy-done.12), channel_id=1, source_target_pairs={{0,4},{4,0},{8,12},{12,8},{16,20},{20,16},{24,28},{28,24},{1,5},{5... | collective-permute-start | bytes 589832 | tf_op jit(solution)/shard_map/ppermute | solution.py:25
  84.9 4.6 %collective-permute-done.7 = bf16[48,2048]{1,0:T(8,128)(2,1)S(1)} collective-permute-done((bf16[48,2048]{1,0:T(8,128)(2,1)}, bf16[48,2048]{1,0:T(8,128)(2,1)S(1)}, u32[]{:S(2)}, u32[]{:S(2)}) %collective-permute-start.7) | collective-permute-done | bytes 196640 | tf_op jit(solution)/shard_map/ppermute | solution.py:25
  91.1 7.0 %collective-permute-done.30 = bf16[48,2048]{1,0:T(8,128)(2,1)S(1)} collective-permute-done((bf16[48,2048]{1,0:T(8,128)(2,1)}, bf16[48,2048]{1,0:T(8,128)(2,1)S(1)}, u32[]{:S(2)}, u32[]{:S(2)}) %collective-permute-start.30) | collective-permute-done | bytes 196640 | tf_op jit(solution)/shard_map/ppermute | solution.py:25
  98.1 2.9 %collective-permute-start.23 = (bf16[48,2048]{1,0:T(8,128)(2,1)}, bf16[48,2048]{1,0:T(8,128)(2,1)S(1)}, u32[]{:S(2)}, u32[]{:S(2)}) collective-permute-start(bf16[48,2048]{1,0:T(8,128)(2,1)} %copy-done.10), channel_id=1, source_target_pairs={{0,20},{4,16},{8,28},{12,24},{16,4},{20,0},{24,12},{28,8},{1,21},{... | collective-permute-start | bytes 589832 | tf_op jit(solution)/shard_map/ppermute | solution.py:25
  101.0 8.8 %collective-permute-done.23 = bf16[48,2048]{1,0:T(8,128)(2,1)S(1)} collective-permute-done((bf16[48,2048]{1,0:T(8,128)(2,1)}, bf16[48,2048]{1,0:T(8,128)(2,1)S(1)}, u32[]{:S(2)}, u32[]{:S(2)}) %collective-permute-start.23) | collective-permute-done | bytes 196640 | tf_op jit(solution)/shard_map/ppermute | solution.py:25
  111.2 6.6 %collective-permute-done.8 = bf16[48,2048]{1,0:T(8,128)(2,1)S(1)} collective-permute-done((bf16[48,2048]{1,0:T(8,128)(2,1)}, bf16[48,2048]{1,0:T(8,128)(2,1)S(1)}, u32[]{:S(2)}, u32[]{:S(2)}) %collective-permute-start.8) | collective-permute-done | bytes 196640 | tf_op jit(solution)/shard_map/ppermute | solution.py:25
  122.2 7.5 %collective-permute-done.24.refs_1_ = bf16[96,2048]{1,0:T(8,128)(2,1)S(1)} collective-permute-done((bf16[96,2048]{1,0:T(8,128)(2,1)S(1)}, bf16[96,2048]{1,0:T(8,128)(2,1)S(1)}, u32[]{:S(2)}, u32[]{:S(2)}) %collective-permute-start.24) | collective-permute-done | bytes 393248 | tf_op jit(solution)/shard_map/ppermute | solution.py:34
  129.8 6.9 %expert_rows.4 = (f32[48,2048]{1,0:T(8,128)S(1)}, f32[48,2048]{1,0:T(8,128)S(1)}, bf16[48,2048]{1,0:T(8,128)(2,1)S(1)}, bf16[48,2048]{1,0:T(8,128)(2,1)S(1)}) custom-call(s32[2]{0:T(128)S(1)} %copy-done.6, bf16[96,2048]{1,0:T(8,128)(2,1)S(1)} %constant_dynamic-update-slice_fusion.3.refs_0_, bf16[96,2048]{1,0:T(8,128)(2,1)S(1)} %collective-permute-done.24.refs_1_, ...), custom_call_target="tpu_custom_call" | custom-call | flops 2415919104 | bytes 12582912 | tf_op jit(solution)/shard_map/expert_rows/pallas_call | solution.py:275
  138.2 6.9 %expert_rows.5 = (f32[96,2048]{1,0:T(8,128)S(1)}, bf16[96,2048]{1,0:T(8,128)(2,1)S(1)}) custom-call(s32[2]{0:T(128)S(1)} %copy-done.6, bf16[96,2048]{1,0:T(8,128)(2,1)S(1)} %constant_dynamic-update-slice_fusion.5.refs_0_, bf16[96,2048]{1,0:T(8,128)(2,1)S(1)} %collective-permute-done.31.refs_1_, bf16[2048,512]{1,0:T(8,128)(2,1)} %bitcast.11.refs_4_.refs_2_, ...), custom_call_target="tpu_custom_call" | custom-call | flops 2415919104 | bytes 12582912 | tf_op jit(solution)/shard_map/expert_rows/pallas_call | solution.py:275
  147.2 12.0 %collective-permute-done.27 = bf16[48,2048]{1,0:T(8,128)(2,1)S(1)} collective-permute-done((bf16[48,2048]{1,0:T(8,128)(2,1)S(1)}, bf16[48,2048]{1,0:T(8,128)(2,1)S(1)}, u32[]{:S(2)}, u32[]{:S(2)}) %collective-permute-start.27) | collective-permute-done | bytes 196640 | tf_op jit(solution)/shard_map/ppermute | solution.py:34
  159.9 8.7 %collective-permute-done.25 = bf16[48,2048]{1,0:T(8,128)(2,1)S(1)} collective-permute-done((bf16[48,2048]{1,0:T(8,128)(2,1)S(1)}, bf16[48,2048]{1,0:T(8,128)(2,1)S(1)}, u32[]{:S(2)}, u32[]{:S(2)}) %collective-permute-start.25) | collective-permute-done | bytes 196640 | tf_op jit(solution)/shard_map/ppermute | solution.py:34
  168.8 9.4 %expert_rows.3 = (f32[48,2048]{1,0:T(8,128)S(1)}, f32[144,2048]{1,0:T(8,128)S(1)}, bf16[48,2048]{1,0:T(8,128)(2,1)S(1)}, bf16[144,2048]{1,0:T(8,128)(2,1)S(1)}) custom-call(s32[2]{0:T(128)S(1)} %copy-done.6, bf16[48,2048]{1,0:T(8,128)(2,1)S(1)} %get-tuple-element.35.refs_0_, bf16[144,2048]{1,0:T(8,128)(2,1)S(1)} %constant_dynamic-update-slice_fusion.refs_1_, ...), custom_call_target="tpu_custom_call" | custom-call | flops 4831838208 | bytes 12582912 | tf_op jit(solution)/shard_map/expert_rows/pallas_call | solution.py:275
  180.3 3.0 %collective-permute-start.33 = (bf16[48,2048]{1,0:T(8,128)(2,1)S(1)}, bf16[48,2048]{1,0:T(8,128)(2,1)S(1)}, u32[]{:S(2)}, u32[]{:S(2)}) collective-permute-start(bf16[48,2048]{1,0:T(8,128)(2,1)S(1)} %get-tuple-element.57), channel_id=1, source_target_pairs={{0,24},{4,28},{8,16},{12,20},{16,8},{20,12},{24,0},{28,4},{1,25},{... | collective-permute-start | bytes 589832 | tf_op jit(solution)/shard_map/ppermute | solution.py:25
  183.3 9.1 %collective-permute-done.18 = bf16[144,2048]{1,0:T(8,128)(2,1)S(1)} collective-permute-done((bf16[144,2048]{1,0:T(8,128)(2,1)S(1)}, bf16[144,2048]{1,0:T(8,128)(2,1)S(1)}, u32[]{:S(2)}, u32[]{:S(2)}) %collective-permute-start.18) | collective-permute-done | bytes 589856 | tf_op jit(solution)/shard_map/ppermute | solution.py:34
  192.4 2.6 %collective-permute-start.34 = (bf16[48,2048]{1,0:T(8,128)(2,1)S(1)}, bf16[48,2048]{1,0:T(8,128)(2,1)S(1)}, u32[]{:S(2)}, u32[]{:S(2)}) collective-permute-start(bf16[48,2048]{1,0:T(8,128)(2,1)S(1)} %get-tuple-element.56), channel_id=1, source_target_pairs={{0,28},{4,24},{8,20},{12,16},{16,12},{20,8},{24,4},{28,0},{1,29},{... | collective-permute-start | bytes 589832 | tf_op jit(solution)/shard_map/ppermute | solution.py:25
  195.1 2.1 %collective-permute-start.19 = (bf16[48,2048]{1,0:T(8,128)(2,1)S(1)}, bf16[48,2048]{1,0:T(8,128)(2,1)S(1)}, u32[]{:S(2)}, u32[]{:S(2)}) collective-permute-start(bf16[48,2048]{1,0:T(8,128)(2,1)S(1)} %get-tuple-element.55), channel_id=1, source_target_pairs={{0,4},{4,0},{8,12},{12,8},{16,20},{20,16},{24,28},{28,24},{1,5},{5... | collective-permute-start | bytes 589832 | tf_op jit(solution)/shard_map/ppermute | solution.py:25
  198.8 2.1 %collective-permute-done.34.refs_7_ = bf16[48,2048]{1,0:T(8,128)(2,1)S(1)} collective-permute-done((bf16[48,2048]{1,0:T(8,128)(2,1)S(1)}, bf16[48,2048]{1,0:T(8,128)(2,1)S(1)}, u32[]{:S(2)}, u32[]{:S(2)}) %collective-permute-start.34) | collective-permute-done | bytes 196640 | tf_op jit(solution)/shard_map/ppermute | solution.py:25
  202.9 2.2 %collective-permute-done.21.refs_3_ = bf16[48,2048]{1,0:T(8,128)(2,1)S(1)} collective-permute-done((bf16[48,2048]{1,0:T(8,128)(2,1)S(1)}, bf16[48,2048]{1,0:T(8,128)(2,1)S(1)}, u32[]{:S(2)}, u32[]{:S(2)}) %collective-permute-start.21) | collective-permute-done | bytes 196640 | tf_op jit(solution)/shard_map/ppermute | solution.py:25
  (122 shorter events, 42.2 us)
Async XLA Ops:
  0.7 10.5 %collective-permute-start = (bf16[8,512]{1,0:T(8,128)(2,1)S(1)}, bf16[8,512]{1,0:T(8,128)(2,1)S(1)}, u32[]{:S(2)}, u32[]{:S(2)}) collective-permute-start(bf16[8,512]{1,0:T(8,128)(2,1)S(1)} %slice.63), channel_id=1, source_target_pairs={{0,4},{4,8},{8,12},{12,16},{16,20},{20,24},{24,28},{1,5},{5,9},{9,... | collective-permute-start | bytes 24584 | tf_op jit(solution)/shard_map/ppermute | solution.py:21
  5.6 32.9 %collective-permute-start.5 = (bf16[512,2048]{1,0:T(8,128)(2,1)}, bf16[512,2048]{1,0:T(8,128)(2,1)}, u32[]{:S(2)}, u32[]{:S(2)}) collective-permute-start(bf16[512,2048]{1,0:T(8,128)(2,1)} %param.23), channel_id=1, source_target_pairs={{0,1},{1,0},{2,3},{3,2},{4,5},{5,4},{6,7},{7,6},{8,9},{9,8},{10,11... | collective-permute-start | bytes 6291464 | tf_op jit(solution)/shard_map/ppermute | solution.py:29
  8.0 57.1 %collective-permute-start.15 = (bf16[1024,512]{1,0:T(8,128)(2,1)}, bf16[1024,512]{1,0:T(8,128)(2,1)S(1)}, u32[]{:S(2)}, u32[]{:S(2)}) collective-permute-start(bf16[1024,512]{1,0:T(8,128)(2,1)} %dynamic-slice_bitcast_fusion), channel_id=1, source_target_pairs={{0,2},{1,3},{2,0},{3,1},{4,6},{5,7},{6,4},{7,5},{8,10},{9,11},{10,... | collective-permute-start | bytes 3145736 | tf_op jit(solution)/shard_map/ppermute | solution.py:34
  9.5 110.6 %collective-permute-start.12 = (bf16[2048,512]{1,0:T(8,128)(2,1)}, bf16[2048,512]{1,0:T(8,128)(2,1)}, u32[]{:S(2)}, u32[]{:S(2)}) collective-permute-start(bf16[2048,512]{1,0:T(8,128)(2,1)} %bitcast.11.refs_4_.refs_2_), channel_id=1, source_target_pairs={{0,1},{1,0},{2,3},{3,2},{4,5},{5,4},{6,7},{7,6},{8,9},{9,8},{10,11... | collective-permute-start | bytes 6291464 | tf_op jit(solution)/shard_map/ppermute | solution.py:29
  9.7 112.0 %collective-permute-start.13 = (bf16[2048,512]{1,0:T(8,128)(2,1)}, bf16[2048,512]{1,0:T(8,128)(2,1)}, u32[]{:S(2)}, u32[]{:S(2)}) collective-permute-start(bf16[2048,512]{1,0:T(8,128)(2,1)} %bitcast.12.refs_5_.refs_3_), channel_id=1, source_target_pairs={{0,1},{1,0},{2,3},{3,2},{4,5},{5,4},{6,7},{7,6},{8,9},{9,8},{10,11... | collective-permute-start | bytes 6291464 | tf_op jit(solution)/shard_map/ppermute | solution.py:29
  27.8 4.6 %collective-permute-start.3 = (f32[2,512]{1,0:T(2,128)S(1)}, f32[2,512]{1,0:T(2,128)S(1)}, u32[]{:S(2)}, u32[]{:S(2)}) collective-permute-start(f32[2,512]{1,0:T(2,128)S(1)} %pad_maximum_fusion.1), channel_id=1, source_target_pairs={{0,16},{4,20},{8,24},{12,28},{16,0},{20,4},{24,8},{28,12},{1,17},{... | collective-permute-start | bytes 12296 | tf_op jit(solution)/shard_map/ppermute | solution.py:25
  38.0 84.2 %collective-permute-start.14 = (bf16[2048,512]{1,0:T(8,128)(2,1)S(1)}, bf16[2048,512]{1,0:T(8,128)(2,1)}, u32[]{:S(2)}, u32[]{:S(2)}) collective-permute-start(bf16[2048,512]{1,0:T(8,128)(2,1)S(1)} %bitcast.34), channel_id=1, source_target_pairs={{0,1},{1,0},{2,3},{3,2},{4,5},{5,4},{6,7},{7,6},{8,9},{9,8},{10,11... | collective-permute-start | bytes 6291464 | tf_op jit(solution)/shard_map/ppermute | solution.py:29
  40.8 13.9 %collective-permute-start.6 = (bf16[128,2048]{1,0:T(8,128)(2,1)S(1)}, bf16[128,2048]{1,0:T(8,128)(2,1)S(1)}, u32[]{:S(2)}, u32[]{:S(2)}) collective-permute-start(bf16[128,2048]{1,0:T(8,128)(2,1)S(1)} %fusion), channel_id=1, source_target_pairs={{0,2},{1,3},{2,0},{3,1},{4,6},{5,7},{6,4},{7,5},{8,10},{9,11},{10,... | collective-permute-start | bytes 1572872 | tf_op jit(solution)/shard_map/ppermute | solution.py:34
  61.1 8.3 %collective-permute-start.29 = (bf16[48,2048]{1,0:T(8,128)(2,1)}, bf16[48,2048]{1,0:T(8,128)(2,1)}, u32[]{:S(2)}, u32[]{:S(2)}) collective-permute-start(bf16[48,2048]{1,0:T(8,128)(2,1)} %get-tuple-element.49), channel_id=1, source_target_pairs={{0,24},{4,28},{8,16},{12,20},{16,8},{20,12},{24,0},{28,4},{1,25},{... | collective-permute-start | bytes 589832 | tf_op jit(solution)/shard_map/ppermute | solution.py:25
  65.0 44.8 %collective-permute-start.16 = (bf16[1024,512]{1,0:T(8,128)(2,1)S(1)}, bf16[1024,512]{1,0:T(8,128)(2,1)S(1)}, u32[]{:S(2)}, u32[]{:S(2)}) collective-permute-start(bf16[1024,512]{1,0:T(8,128)(2,1)S(1)} %collective-permute-done.15.refs_10_.refs_8_), channel_id=1, source_target_pairs={{0,1},{1,0},{2,3},{3,2},{4,5},{5,4},{6,7},{7,6},{8,9},{9,8},{10,11... | collective-permute-start | bytes 3145736 | tf_op jit(solution)/shard_map/ppermute | solution.py:29
  69.4 12.6 %collective-permute-start.22 = (bf16[48,2048]{1,0:T(8,128)(2,1)}, bf16[48,2048]{1,0:T(8,128)(2,1)S(1)}, u32[]{:S(2)}, u32[]{:S(2)}) collective-permute-start(bf16[48,2048]{1,0:T(8,128)(2,1)} %copy-done.13), channel_id=1, source_target_pairs={{0,16},{4,20},{8,24},{12,28},{16,0},{20,4},{24,8},{28,12},{1,17},{... | collective-permute-start | bytes 589832 | tf_op jit(solution)/shard_map/ppermute | solution.py:25
  82.0 7.5 %collective-permute-start.7 = (bf16[48,2048]{1,0:T(8,128)(2,1)}, bf16[48,2048]{1,0:T(8,128)(2,1)S(1)}, u32[]{:S(2)}, u32[]{:S(2)}) collective-permute-start(bf16[48,2048]{1,0:T(8,128)(2,1)} %copy-done.12), channel_id=1, source_target_pairs={{0,4},{4,0},{8,12},{12,8},{16,20},{20,16},{24,28},{28,24},{1,5},{5... | collective-permute-start | bytes 589832 | tf_op jit(solution)/shard_map/ppermute | solution.py:25
  89.5 8.6 %collective-permute-start.30 = (bf16[48,2048]{1,0:T(8,128)(2,1)}, bf16[48,2048]{1,0:T(8,128)(2,1)S(1)}, u32[]{:S(2)}, u32[]{:S(2)}) collective-permute-start(bf16[48,2048]{1,0:T(8,128)(2,1)} %copy-done.11), channel_id=1, source_target_pairs={{0,28},{4,24},{8,20},{12,16},{16,12},{20,8},{24,4},{28,0},{1,29},{... | collective-permute-start | bytes 589832 | tf_op jit(solution)/shard_map/ppermute | solution.py:25
  98.1 11.7 %collective-permute-start.23 = (bf16[48,2048]{1,0:T(8,128)(2,1)}, bf16[48,2048]{1,0:T(8,128)(2,1)S(1)}, u32[]{:S(2)}, u32[]{:S(2)}) collective-permute-start(bf16[48,2048]{1,0:T(8,128)(2,1)} %copy-done.10), channel_id=1, source_target_pairs={{0,20},{4,16},{8,28},{12,24},{16,4},{20,0},{24,12},{28,8},{1,21},{... | collective-permute-start | bytes 589832 | tf_op jit(solution)/shard_map/ppermute | solution.py:25
  109.8 8.0 %collective-permute-start.8 = (bf16[48,2048]{1,0:T(8,128)(2,1)}, bf16[48,2048]{1,0:T(8,128)(2,1)S(1)}, u32[]{:S(2)}, u32[]{:S(2)}) collective-permute-start(bf16[48,2048]{1,0:T(8,128)(2,1)} %copy-done.9), channel_id=1, source_target_pairs={{0,8},{4,12},{8,0},{12,4},{16,24},{20,28},{24,16},{28,20},{1,9},{5... | collective-permute-start | bytes 589832 | tf_op jit(solution)/shard_map/ppermute | solution.py:25
  109.8 9.7 %collective-permute-start.9 = (bf16[48,2048]{1,0:T(8,128)(2,1)S(1)}, bf16[48,2048]{1,0:T(8,128)(2,1)S(1)}, u32[]{:S(2)}, u32[]{:S(2)}) collective-permute-start(bf16[48,2048]{1,0:T(8,128)(2,1)S(1)} %copy-done.8), channel_id=1, source_target_pairs={{0,12},{4,8},{8,4},{12,0},{16,28},{20,24},{24,20},{28,16},{1,13},{... | collective-permute-start | bytes 589832 | tf_op jit(solution)/shard_map/ppermute | solution.py:25
  117.8 12.0 %collective-permute-start.24 = (bf16[96,2048]{1,0:T(8,128)(2,1)S(1)}, bf16[96,2048]{1,0:T(8,128)(2,1)S(1)}, u32[]{:S(2)}, u32[]{:S(2)}) collective-permute-start(bf16[96,2048]{1,0:T(8,128)(2,1)S(1)} %constant_dynamic-update-slice_fusion.3.refs_0_), channel_id=1, source_target_pairs={{0,2},{1,3},{2,0},{3,1},{4,6},{5,7},{6,4},{7,5},{8,10},{9,11},{10,... | collective-permute-start | bytes 1179656 | tf_op jit(solution)/shard_map/ppermute | solution.py:34
  119.5 18.7 %collective-permute-start.31 = (bf16[96,2048]{1,0:T(8,128)(2,1)S(1)}, bf16[96,2048]{1,0:T(8,128)(2,1)S(1)}, u32[]{:S(2)}, u32[]{:S(2)}) collective-permute-start(bf16[96,2048]{1,0:T(8,128)(2,1)S(1)} %constant_dynamic-update-slice_fusion.5.refs_0_), channel_id=1, source_target_pairs={{0,2},{1,3},{2,0},{3,1},{4,6},{5,7},{6,4},{7,5},{8,10},{9,11},{10,... | collective-permute-start | bytes 1179656 | tf_op jit(solution)/shard_map/ppermute | solution.py:34
  120.1 48.6 %collective-permute-start.10 = (bf16[48,2048]{1,0:T(8,128)(2,1)S(1)}, bf16[48,2048]{1,0:T(8,128)(2,1)S(1)}, u32[]{:S(2)}, u32[]{:S(2)}) collective-permute-start(bf16[48,2048]{1,0:T(8,128)(2,1)S(1)} %get-tuple-element.35.refs_0_), channel_id=1, source_target_pairs={{0,2},{1,3},{2,0},{3,1},{4,6},{5,7},{6,4},{7,5},{8,10},{9,11},{10,... | collective-permute-start | bytes 589832 | tf_op jit(solution)/shard_map/ppermute | solution.py:34
  121.7 47.1 %collective-permute-start.11 = (bf16[144,2048]{1,0:T(8,128)(2,1)S(1)}, bf16[144,2048]{1,0:T(8,128)(2,1)S(1)}, u32[]{:S(2)}, u32[]{:S(2)}) collective-permute-start(bf16[144,2048]{1,0:T(8,128)(2,1)S(1)} %constant_dynamic-update-slice_fusion.refs_1_), channel_id=1, source_target_pairs={{0,2},{1,3},{2,0},{3,1},{4,6},{5,7},{6,4},{7,5},{8,10},{9,11},{10,... | collective-permute-start | bytes 1769480 | tf_op jit(solution)/shard_map/ppermute | solution.py:34
  136.7 22.6 %collective-permute-start.27 = (bf16[48,2048]{1,0:T(8,128)(2,1)S(1)}, bf16[48,2048]{1,0:T(8,128)(2,1)S(1)}, u32[]{:S(2)}, u32[]{:S(2)}) collective-permute-start(bf16[48,2048]{1,0:T(8,128)(2,1)S(1)} %get-tuple-element.48), channel_id=1, source_target_pairs={{0,2},{1,3},{2,0},{3,1},{4,6},{5,7},{6,4},{7,5},{8,10},{9,11},{10,... | collective-permute-start | bytes 589832 | tf_op jit(solution)/shard_map/ppermute | solution.py:34
  145.1 35.1 %collective-permute-start.32 = (bf16[96,2048]{1,0:T(8,128)(2,1)S(1)}, bf16[96,2048]{1,0:T(8,128)(2,1)S(1)}, u32[]{:S(2)}, u32[]{:S(2)}) collective-permute-start(bf16[96,2048]{1,0:T(8,128)(2,1)S(1)} %get-tuple-element.52), channel_id=1, source_target_pairs={{0,2},{1,3},{2,0},{3,1},{4,6},{5,7},{6,4},{7,5},{8,10},{9,11},{10,... | collective-permute-start | bytes 1179656 | tf_op jit(solution)/shard_map/ppermute | solution.py:34
  145.8 22.8 %collective-permute-start.25 = (bf16[48,2048]{1,0:T(8,128)(2,1)S(1)}, bf16[48,2048]{1,0:T(8,128)(2,1)S(1)}, u32[]{:S(2)}, u32[]{:S(2)}) collective-permute-start(bf16[48,2048]{1,0:T(8,128)(2,1)S(1)} %get-tuple-element.46), channel_id=1, source_target_pairs={{0,2},{1,3},{2,0},{3,1},{4,6},{5,7},{6,4},{7,5},{8,10},{9,11},{10,... | collective-permute-start | bytes 589832 | tf_op jit(solution)/shard_map/ppermute | solution.py:34
  159.3 35.8 %collective-permute-start.28 = (bf16[48,2048]{1,0:T(8,128)(2,1)S(1)}, bf16[48,2048]{1,0:T(8,128)(2,1)S(1)}, u32[]{:S(2)}, u32[]{:S(2)}) collective-permute-start(bf16[48,2048]{1,0:T(8,128)(2,1)S(1)} %add_convert_fusion.2), channel_id=1, source_target_pairs={{0,20},{4,16},{8,28},{12,24},{16,4},{20,0},{24,12},{28,8},{1,21},{... | collective-permute-start | bytes 589832 | tf_op jit(solution)/shard_map/ppermute | solution.py:25
  168.7 28.6 %collective-permute-start.26 = (bf16[48,2048]{1,0:T(8,128)(2,1)S(1)}, bf16[48,2048]{1,0:T(8,128)(2,1)S(1)}, u32[]{:S(2)}, u32[]{:S(2)}) collective-permute-start(bf16[48,2048]{1,0:T(8,128)(2,1)S(1)} %add_convert_fusion.3), channel_id=1, source_target_pairs={{0,16},{4,20},{8,24},{12,28},{16,0},{20,4},{24,8},{28,12},{1,17},{... | collective-permute-start | bytes 589832 | tf_op jit(solution)/shard_map/ppermute | solution.py:25
  178.1 14.2 %collective-permute-start.18 = (bf16[144,2048]{1,0:T(8,128)(2,1)S(1)}, bf16[144,2048]{1,0:T(8,128)(2,1)S(1)}, u32[]{:S(2)}, u32[]{:S(2)}) collective-permute-start(bf16[144,2048]{1,0:T(8,128)(2,1)S(1)} %get-tuple-element.42), channel_id=1, source_target_pairs={{0,2},{1,3},{2,0},{3,1},{4,6},{5,7},{6,4},{7,5},{8,10},{9,11},{10,... | collective-permute-start | bytes 1769480 | tf_op jit(solution)/shard_map/ppermute | solution.py:34
  178.8 18.5 %collective-permute-start.17 = (bf16[48,2048]{1,0:T(8,128)(2,1)S(1)}, bf16[48,2048]{1,0:T(8,128)(2,1)S(1)}, u32[]{:S(2)}, u32[]{:S(2)}) collective-permute-start(bf16[48,2048]{1,0:T(8,128)(2,1)S(1)} %get-tuple-element.40), channel_id=1, source_target_pairs={{0,2},{1,3},{2,0},{3,1},{4,6},{5,7},{6,4},{7,5},{8,10},{9,11},{10,... | collective-permute-start | bytes 589832 | tf_op jit(solution)/shard_map/ppermute | solution.py:34
  180.3 18.5 %collective-permute-start.33 = (bf16[48,2048]{1,0:T(8,128)(2,1)S(1)}, bf16[48,2048]{1,0:T(8,128)(2,1)S(1)}, u32[]{:S(2)}, u32[]{:S(2)}) collective-permute-start(bf16[48,2048]{1,0:T(8,128)(2,1)S(1)} %get-tuple-element.57), channel_id=1, source_target_pairs={{0,24},{4,28},{8,16},{12,20},{16,8},{20,12},{24,0},{28,4},{1,25},{... | collective-permute-start | bytes 589832 | tf_op jit(solution)/shard_map/ppermute | solution.py:25
  192.4 8.6 %collective-permute-start.34 = (bf16[48,2048]{1,0:T(8,128)(2,1)S(1)}, bf16[48,2048]{1,0:T(8,128)(2,1)S(1)}, u32[]{:S(2)}, u32[]{:S(2)}) collective-permute-start(bf16[48,2048]{1,0:T(8,128)(2,1)S(1)} %get-tuple-element.56), channel_id=1, source_target_pairs={{0,28},{4,24},{8,20},{12,16},{16,12},{20,8},{24,4},{28,0},{1,29},{... | collective-permute-start | bytes 589832 | tf_op jit(solution)/shard_map/ppermute | solution.py:25
  195.1 7.8 %collective-permute-start.19 = (bf16[48,2048]{1,0:T(8,128)(2,1)S(1)}, bf16[48,2048]{1,0:T(8,128)(2,1)S(1)}, u32[]{:S(2)}, u32[]{:S(2)}) collective-permute-start(bf16[48,2048]{1,0:T(8,128)(2,1)S(1)} %get-tuple-element.55), channel_id=1, source_target_pairs={{0,4},{4,0},{8,12},{12,8},{16,20},{20,16},{24,28},{28,24},{1,5},{5... | collective-permute-start | bytes 589832 | tf_op jit(solution)/shard_map/ppermute | solution.py:25
  197.2 5.7 %collective-permute-start.20 = (bf16[48,2048]{1,0:T(8,128)(2,1)S(1)}, bf16[48,2048]{1,0:T(8,128)(2,1)S(1)}, u32[]{:S(2)}, u32[]{:S(2)}) collective-permute-start(bf16[48,2048]{1,0:T(8,128)(2,1)S(1)} %get-tuple-element.54), channel_id=1, source_target_pairs={{0,8},{4,12},{8,0},{12,4},{16,24},{20,28},{24,16},{28,20},{1,9},{5... | collective-permute-start | bytes 589832 | tf_op jit(solution)/shard_map/ppermute | solution.py:25
  197.3 7.8 %collective-permute-start.21 = (bf16[48,2048]{1,0:T(8,128)(2,1)S(1)}, bf16[48,2048]{1,0:T(8,128)(2,1)S(1)}, u32[]{:S(2)}, u32[]{:S(2)}) collective-permute-start(bf16[48,2048]{1,0:T(8,128)(2,1)S(1)} %get-tuple-element.53), channel_id=1, source_target_pairs={{0,12},{4,8},{8,4},{12,0},{16,28},{20,24},{24,20},{28,16},{1,13},{... | collective-permute-start | bytes 589832 | tf_op jit(solution)/shard_map/ppermute | solution.py:25
  (21 other events, 204.8 us)
where the time goes:
time: 207 us
  waiting for transfers between devices  99.7 us (48%)
  starting transfers between devices  49.2 us (24%)
  Pallas kernels  37 us (18%)
  local copies, waits for them, and re-layouts  10.5 us (5%)
  matrix products  7.11 us (3%)
  other arithmetic  2.95 us (1%)
    ppermute x17, waiting for transfers between devices, across(): lax.ppermute(block, 'sp', [(i, i ^ bits) for i in range(lax.axis_size('sp...  50.8 us
    ppermute x11, waiting for transfers between devices, turned(): lax.ppermute(block, 'tp', [(i, (i + 2 * distance) % size) for i in range(...  48.9 us
    ppermute x17, starting transfers between devices, across(): lax.ppermute(block, 'sp', [(i, i ^ bits) for i in range(lax.axis_size('sp...  33 us
    pallas_call x3, Pallas kernels, expert_rows(): pl.pallas_call(functools.partial(expert_kernel, groups=len(rows), outs=le...  23.2 us
    ppermute x11, starting transfers between devices, turned(): lax.ppermute(block, 'tp', [(i, (i + 2 * distance) % size) for i in range(...  10.2 us
    pallas_call x1, Pallas kernels, local_scan(): pl.pallas_call(scan_kernel, grid=(channels // lanes,), in_specs=[column(r...  7.63 us
    unnamed x42, local copies, waits for them, and re-layouts  6.74 us
    ppermute x1, starting transfers between devices, shifted(): return lax.ppermute(block, 'sp', [(i, i + 1) for i in range(size - 1)])  4.86 us
  transfers between devices with their start and end apart: 35, of which 19 were waited for; matrix products, arithmetic and copies ran while one was open for 7% of the time, Pallas kernels for 17%

commit v1 on v0

--- a/solution.py
+++ b/solution.py
@@ -36,6 +36,7 @@
 
 LANES = 128
 GROUPS = 2
+GRANT = 12
 SEGMENTS = 8
 
 
@@ -48,7 +49,29 @@
     return jnp.concatenate(rows, axis=0)
 
 
-def scan_kernel(rim, x, taps, recur, inward, slope, boost, local, running, total, wide, decays, drives):
+def scan_kernel(place, rim, x, taps, recur, inward, slope, boost, down, local, running, total, *refs):
+    *halves, wide, decays, drives, held, cut, kept = refs
+    pairs = len(halves) // 2 + 1
+    rows = halves[0].shape[0]
+    loads, stores = [], []
+    for i, half in enumerate(halves):
+        target = lax.rem(place[0] + i // 2 + 1, pairs)
+        begin = pl.multiple_of((2 * target + i % 2) * rows, rows)
+        loads.append(pltpu.make_async_copy(down.at[pl.ds(begin, rows)], held.at[i], cut.at[i]))
+        stores.append(pltpu.make_async_copy(held.at[i], half, kept.at[i]))
+    final = pl.program_id(0) == pl.num_programs(0) - 1
+
+    @pl.when(pl.program_id(0) == 0)
+    def _():
+        for copy in loads:
+            copy.start()
+
+    @pl.when(final)
+    def _():
+        for load, store in zip(loads, stores):
+            load.wait()
+            store.start()
+
     tokens, _ = x.shape
     margin = rim.shape[0]
     count = taps.shape[0]
@@ -100,13 +123,21 @@
         total[0:1, g * width : (g + 1) * width] = a
         total[1:2, g * width : (g + 1) * width] = b
 
-
-def local_scan(rim, x, taps, recur, inward, slope, boost):
+    @pl.when(final)
+    def _():
+        for store in stores:
+            store.wait()
+
+
+def local_scan(place, rim, x, taps, recur, inward, slope, boost, down, pairs):
     tokens, channels = x.shape
     groups = min(GROUPS, channels // LANES)
     lanes = groups * LANES
     width = recur.shape[1]
     folded = pl.BlockSpec((groups, tokens, LANES), lambda i: (i, 0, 0))
+    anywhere = pl.BlockSpec(memory_space=pl.ANY)
+    count = 2 * (pairs - 1)
+    half = jax.ShapeDtypeStruct((down.shape[0] // (2 * pairs), down.shape[1]), down.dtype)
     column = lambda rows: pl.BlockSpec((rows, lanes), lambda i: (0, i))
     blocks = pl.BlockSpec((lanes // width, width, width), lambda i: (i, 0, 0))
     wide = jax.ShapeDtypeStruct((channels // LANES, tokens, LANES), jnp.float32)
@@ -114,6 +145,7 @@
         scan_kernel,
         grid=(channels // lanes,),
         in_specs=[
+            pl.BlockSpec(memory_space=pltpu.SMEM),
             column(rim.shape[0]),
             column(tokens),
             column(taps.shape[0]),
@@ -121,16 +153,20 @@
             blocks,
             column(1),
             column(tokens),
+            anywhere,
         ],
-        out_specs=[folded, folded, column(2)],
-        out_shape=[wide, wide, jax.ShapeDtypeStruct((2, channels), jnp.float32)],
+        out_specs=[folded, folded, column(2)] + [anywhere] * count,
+        out_shape=[wide, wide, jax.ShapeDtypeStruct((2, channels), jnp.float32)] + [half] * count,
         scratch_shapes=[
             pltpu.VMEM((tokens + rim.shape[0], lanes), jnp.float32),
             pltpu.VMEM((groups, tokens, LANES), jnp.float32),
             pltpu.VMEM((groups, tokens, LANES), jnp.float32),
+            pltpu.VMEM((count, *half.shape), half.dtype),
+            pltpu.SemaphoreType.DMA((count,)),
+            pltpu.SemaphoreType.DMA((count,)),
         ],
         name="local_scan",
-    )(rim, x, taps, recur, inward, slope, boost)
+    )(place, rim, x, taps, recur, inward, slope, boost, down)
 
 
 def branch_kernel(place, entering, local, running, gate, keep, give):
@@ -232,10 +268,11 @@
 
 def expert_kernel(place, *refs, groups, outs, pairs):
     rows_in, refs = refs[:groups], refs[groups:]
-    (gate_own, up_own, gate_far, up_far, *downs), refs = refs[: 4 + 2 * pairs], refs[4 + 2 * pairs :]
+    used = 2 + 4 * pairs
+    (gate_own, up_own, gate_far, up_far, *downs), refs = refs[:used], refs[used:]
     rows_out, (left, active) = refs[:outs], refs[outs:]
     hidden = gate_own.shape[1]
-    strip, width = 2 * hidden, downs[0].shape[1]
+    width = downs[0].shape[1]
     at = 0
     for block in rows_in:
         left[at : at + block.shape[0], :] = block[...]
@@ -249,33 +286,36 @@
             upward = jnp.dot(left[...], ups[:, here], preferred_element_type=jnp.float32)
             there = pl.ds(pl.multiple_of(core * hidden + start, step), step)
             active[:, there] = (jax.nn.silu(gate) * upward).astype(jnp.bfloat16)
-    for i, down in enumerate(downs):
-        if i < 2:
-            side, d = i, 0
-            piece = down[pl.ds(pl.multiple_of(place[0] * strip, strip), strip), :]
-        else:
-            side, d = (i - 2) // (pairs - 1), (i - 2) % (pairs - 1) + 1
-            piece = down[...]
-        core = place[1] if side == 0 else 1 - place[1]
-        column = (lax.rem(place[0] - d + pairs, pairs) * 2 + core) * width
-        there = pl.ds(pl.multiple_of(column, width), width)
-        result = jnp.dot(active[...], piece, preferred_element_type=jnp.float32)
-        at = 0
-        for block in rows_out:
-            block[:, there] = result[at : at + block.shape[0]].astype(block.dtype)
-            at += block.shape[0]
+    for side in range(2):
+        for d in range(pairs):
+            core = place[1] if side == 0 else 1 - place[1]
+            column = (lax.rem(place[0] - d + pairs, pairs) * 2 + core) * width
+            there = pl.ds(pl.multiple_of(column, width), width)
+            if d == 0:
+                begin = pl.multiple_of(place[0] * 2 * hidden, 2 * hidden)
+                piece = downs[side][pl.ds(begin, 2 * hidden), :]
+                result = jnp.dot(active[...], piece, preferred_element_type=jnp.float32)
+            else:
+                first, second = downs[2 + 2 * (pairs - 1) * side + 2 * d - 2 :][:2]
+                result = jnp.dot(
+                    active[:, :hidden], first[...], preferred_element_type=jnp.float32
+                ) + jnp.dot(active[:, hidden:], second[...], preferred_element_type=jnp.float32)
+            at = 0
+            for block in rows_out:
+                block[:, there] = result[at : at + block.shape[0]].astype(block.dtype)
+                at += block.shape[0]
 
 
 def expert_rows(place, rows, outs, weights):
     *gates, downs = weights
     model, hidden = gates[0].shape
-    pairs = len(downs) // 2
+    pairs = (len(downs) + 2) // 4
     height = sum(a.shape[0] for a in rows)
     vmem = pl.BlockSpec(memory_space=pltpu.VMEM)
     return pl.pallas_call(
         functools.partial(expert_kernel, groups=len(rows), outs=len(outs), pairs=pairs),
         in_specs=[pl.BlockSpec(memory_space=pltpu.SMEM)]
-        + [vmem] * (len(rows) + 4 + 2 * pairs),
+        + [vmem] * (len(rows) + 4 + len(downs)),
         out_specs=[vmem] * len(outs),
         out_shape=[jax.ShapeDtypeStruct((count, model), kind) for count, kind in outs],
         scratch_shapes=[
@@ -287,9 +327,33 @@
             bytes_accessed=12 * model * hidden,
             transcendentals=0,
         ),
-        compiler_params=granted(28),
+        compiler_params=granted(GRANT),
         name="expert_rows",
     )(place, *rows, *gates, *downs)
+
+
+def sum_kernel(own, *refs, pieces):
+    backs, blocks = refs[:pieces], refs[pieces:]
+    total = own[...]
+    for back in backs:
+        total = total + back[...].astype(jnp.float32)
+    height = blocks[0].shape[0]
+    for i, block in enumerate(blocks):
+        block[...] = total[i * height : (i + 1) * height].astype(jnp.bfloat16)
+
+
+def sum_rows(own, backs, count):
+    rows, width = own.shape
+    block = jax.ShapeDtypeStruct((rows // count, width), jnp.bfloat16)
+    return pl.pallas_call(
+        functools.partial(sum_kernel, pieces=len(backs)),
+        out_shape=[block] * count,
+        cost_estimate=pl.CostEstimate(
+            flops=2 * rows * width, bytes_accessed=8 * rows * width, transcendentals=0
+        ),
+        compiler_params=granted(8),
+        name="sum_rows",
+    )(own, *backs)
 
 
 def mix_kernel(slots, pair_weight, mix):
@@ -397,17 +461,9 @@
     capacity = max(2, 3 * rows_dev // experts)
 
     gate_own, up_own, down_all = gate_weight[0], up_weight[0], down_weight[0]
-    strip = down_all.shape[0] // pairs
-    strip_of = lambda d: lax.dynamic_slice_in_dim(down_all, lax.rem(row + d, pairs) * strip, strip, 0)
     rim = shifted(recurrent_input[tokens_here - 8 :])
-    down_own = [turned(strip_of(d), d) for d in range(1, pairs)]
-    projection_far = swapped(output_projection_weight)
-    gate_far, up_far = swapped(gate_own), swapped(up_own)
-    down_far = [swapped(piece) for piece in down_own]
-    down_whole = [down_all, swapped(down_all)]
-    weights = (gate_own, up_own, gate_far, up_far, down_whole + down_own + down_far)
-
-    local, running, total = local_scan(
+    local, running, total, *halves = local_scan(
+        place,
         rim,
         recurrent_input,
         filter_weight,
@@ -415,7 +471,18 @@
         input_gate_matrix,
         channel_decay_raw[None, :],
         token_decay_boost,
+        down_all,
+        pairs,
     )
+    projection_far = swapped(output_projection_weight)
+    gate_far, up_far = swapped(gate_own), swapped(up_own)
+    down_own, down_far = [], []
+    for d in range(1, pairs):
+        for h in range(2):
+            down_own.append(turned(halves[2 * d - 2 + h], d))
+            down_far.append(swapped(down_own[-1]))
+    down_whole = [down_all, swapped(down_all)]
+    weights = (gate_own, up_own, gate_far, up_far, down_whole + down_own + down_far)
 
     own_routes = lax.dynamic_slice_in_dim(routes, column * rows_dev, rows_dev, 0)
     own_flat, own_rank = slot_numbers(own_routes, experts)
@@ -443,54 +510,37 @@
     arrived = {0: blocks[0]}
     for k in range(1, experts):
         arrived[k] = across(blocks[k], k)
-    own = [jnp.concatenate([arrived[k] for k in range(*cut)], axis=0) for cut in cuts]
+    own = [joined([arrived[k] for k in range(*cut)]) for cut in cuts]
     theirs = [[turned(g, d) for d in range(1, pairs)] for g in own]
     hops = range(1, pairs)
-    splits = return_cuts(experts)
-
-    def run(chosen):
+    sizes = [(cut[1] - cut[0]) * capacity for cut in cuts]
+    returned = {}
+    near, mid = len(cuts) // 2, 3 * len(cuts) // 4
+    calls = [(0, near), (near, mid), (mid, len(cuts))]
+    for first, end in calls:
+        chosen = range(first, end)
         rows = [own[i] for i in chosen] + [g for i in chosen for g in theirs[i]]
-        outs = []
-        for kind, count in ((jnp.float32, 1), (jnp.bfloat16, pairs - 1)):
-            for i in chosen:
-                parts = [((b - a) * capacity, kind) for a, b in splits if cuts[i][0] <= a < cuts[i][1]]
-                outs += parts * count
-        results = iter(expert_rows(place, rows, outs, weights))
-        wide = {s: next(results) for i in chosen for s in inner(i)}
-        narrow = {s: [] for i in chosen for s in inner(i)}
-        for i in chosen:
-            for _ in hops:
-                for s in inner(i):
-                    narrow[s].append(next(results))
-        return wide, narrow
-
-    def inner(i):
-        return [s for s in splits if cuts[i][0] <= s[0] < cuts[i][1]]
-
-    returned = {}
-    for chosen in ((0, 1), (2,), (3,)):
-        wide, narrow = run(chosen)
-        for cut in wide:
-            sums = wide[cut]
-            for d in hops:
-                back = turned(narrow[cut][d - 1], pairs - d)
-                sums = sums + back.astype(jnp.float32)
-            for j, k in enumerate(range(*cut)):
-                result = sums[j * capacity : (j + 1) * capacity].astype(jnp.bfloat16)
+        outs = [(sizes[i], jnp.float32) for i in chosen]
+        outs += [(sizes[i], jnp.bfloat16) for i in chosen for _ in hops]
+        results = expert_rows(place, rows, outs, weights)
+        wide, narrow = results[: len(chosen)], results[len(chosen) :]
+        for j, i in enumerate(chosen):
+            parts = narrow[j * len(hops) : (j + 1) * len(hops)]
+            backs = [turned(part, pairs - d) for part, d in zip(parts, hops)]
+            sums = sum_rows(wide[j], backs, cuts[i][1] - cuts[i][0])
+            for k, result in zip(range(*cuts[i]), sums):
                 returned[k] = across(result, k) if k else result
     mix = mix_weights(slots, expert_pair_weight, experts * padded(capacity))
     return blend_rows(stream, mix, [returned[k] for k in range(experts)])
 
 
+def joined(blocks):
+    return blocks[0] if len(blocks) == 1 else jnp.concatenate(blocks, axis=0)
+
+
 def row_cuts(experts):
-    quarter = experts // 4
-    return [(0, 1), (1, 2 * quarter), (2 * quarter, 3 * quarter), (3 * quarter, experts)]
-
-
-def return_cuts(experts):
-    first, near, far, last = row_cuts(experts)
-    middle = (far[0] + far[1]) // 2
-    return [first, near, (far[0], middle), (middle, far[1]), last]
+    count = max(1, experts // 8)
+    return [(k, k + count) for k in range(0, experts, count)]
 
 
 def solution(mesh):

time: 207 us -> 206 us (level)
  starting transfers between devices: 49.2 us -> 70.4 us
  waiting for transfers between devices: 99.7 us -> 78.5 us
  local copies, waits for them, and re-layouts: 10.5 us -> 7.92 us
  matrix products: 7.11 us -> 9.3 us
    ppermute x11 -> x19, starting transfers between devices: 10.2 us -> 23.2 us  [turned(): lax.ppermute(block, 'tp', [(i, (i + 2 * distance) % size) for i in range(...]
    ppermute x11 -> x19, waiting for transfers between devices: 48.9 us -> 37.3 us  [turned(): lax.ppermute(block, 'tp', [(i, (i + 2 * distance) % size) for i in range(...]
    ppermute x17, waiting for transfers between devices: 50.8 us -> 40 us  [across(): lax.ppermute(block, 'sp', [(i, i ^ bits) for i in range(lax.axis_size('sp...]
    ppermute x17, starting transfers between devices: 33 us -> 41.3 us  [across(): lax.ppermute(block, 'sp', [(i, i ^ bits) for i in range(lax.axis_size('sp...]
    pallas_call x3, Pallas kernels: 23.2 us -> 19.5 us  [expert_rows(): pl.pallas_call(functools.partial(expert_kernel, groups=len(rows), outs=le...]
    dynamic_slice x1 -> x0, local copies, waits for them, and re-layouts: 2.26 us -> none  [body(): lax.dynamic_slice_in_dim(down_all, lax.rem(row + d, pairs) * strip, strip...]
    unnamed x42 -> x44, local copies, waits for them, and re-layouts: 6.74 us -> 5.9 us
    pallas_call x1 -> x9, Pallas kernels: 7.63 us -> 8.03 us  [the longest x1 7.73 us: local_scan(): pl.pallas_call(scan_kernel, grid=(channels // lanes,), in_specs=[pl.Block...]
  transfers between devices with their start and end apart: 35 -> 44, of which waited for: 19 -> 23; matrix products, arithmetic and copies ran while one was open for 7% -> 7% of each run, Pallas kernels for 17% -> 16%
where the time goes in v1:
time: 206 us; the launch traced here: 205 us
  waiting for transfers between devices  78.5 us (38%)
  starting transfers between devices  70.4 us (34%)
  Pallas kernels  35.1 us (17%)
  matrix products  9.3 us (5%)
  local copies, waits for them, and re-layouts  7.92 us (4%)
  other arithmetic  3.7 us (2%)
    ppermute x17, starting transfers between devices, across(): lax.ppermute(block, 'sp', [(i, i ^ bits) for i in range(lax.axis_size('sp...  41.3 us
    ppermute x17, waiting for transfers between devices, across(): lax.ppermute(block, 'sp', [(i, i ^ bits) for i in range(lax.axis_size('sp...  40 us
    ppermute x19, waiting for transfers between devices, turned(): lax.ppermute(block, 'tp', [(i, (i + 2 * distance) % size) for i in range(...  37.3 us
    ppermute x19, starting transfers between devices, turned(): lax.ppermute(block, 'tp', [(i, (i + 2 * distance) % size) for i in range(...  23.2 us
    pallas_call x3, Pallas kernels, expert_rows(): pl.pallas_call(functools.partial(expert_kernel, groups=len(rows), outs=le...  19.5 us
    pallas_call x1, Pallas kernels, local_scan(): pl.pallas_call(scan_kernel, grid=(channels // lanes,), in_specs=[pl.Block...  7.73 us
    unnamed x44, local copies, waits for them, and re-layouts  5.9 us
    dot_general x2, matrix products, projected(): jnp.dot(taken[d], projection_far, preferred_element_type=jnp.float32)  5.14 us
  transfers between devices with their start and end apart: 44, of which 23 were waited for; matrix products, arithmetic and copies ran while one was open for 7% of the time, Pallas kernels for 16%

profile of v1, /device:TPU:0, one launch (start us, length us, event | category | flops | bytes accessed | tf_op | source)
XLA Modules:
  0.0 205.4 jit_solution(11615224331284660303)
XLA Ops:
  1.2 4.4 %collective-permute-start = (bf16[8,512]{1,0:T(8,128)(2,1)S(1)}, bf16[8,512]{1,0:T(8,128)(2,1)S(1)}, u32[]{:S(2)}, u32[]{:S(2)}) collective-permute-start(bf16[8,512]{1,0:T(8,128)(2,1)S(1)} %slice.43), channel_id=1, source_target_pairs={{0,4},{4,8},{8,12},{12,16},{16,20},{20,24},{24,28},{1,5},{5,9},{9,... | collective-permute-start | bytes 24584 | tf_op jit(solution)/shard_map/ppermute | solution.py:21
  7.5 7.7 %local_scan.1 = (f32[4,512,128]{2,1,0:T(8,128)}, f32[4,512,128]{2,1,0:T(8,128)}, f32[2,512]{1,0:T(2,128)}, bf16[512,512]{1,0:T(8,128)(2,1)}, bf16[512,512]{1,0:T(8,128)(2,1)}) custom-call(s32[2]{0:T(128)} %pad_add_fusion.place, bf16[8,512]{1,0:T(8,128)(2,1)} %copy-done.19, bf16[512,512]{1,0:T(8,128)(2,1)} %x.1, f32[4,512]{1,0:T(4,128)} %taps.1, ...), custom_call_target="tpu_custom_call" | custom-call | tf_op jit(solution)/shard_map/local_scan/pallas_call | solution.py:144
  15.3 2.4 %collective-permute-start.1 = (f32[2,512]{1,0:T(2,128)}, f32[2,512]{1,0:T(2,128)S(1)}, u32[]{:S(2)}, u32[]{:S(2)}) collective-permute-start(f32[2,512]{1,0:T(2,128)} %get-tuple-element.37), channel_id=1, source_target_pairs={{0,4},{4,0},{8,12},{12,8},{16,20},{20,16},{24,28},{28,24},{1,5},{5... | collective-permute-start | bytes 12296 | tf_op jit(solution)/shard_map/ppermute | solution.py:25
  20.2 3.1 %collective-permute-start.2 = (f32[2,512]{1,0:T(2,128)S(1)}, f32[2,512]{1,0:T(2,128)S(1)}, u32[]{:S(2)}, u32[]{:S(2)}) collective-permute-start(f32[2,512]{1,0:T(2,128)S(1)} %pad_maximum_fusion), channel_id=1, source_target_pairs={{0,8},{4,12},{8,0},{12,4},{16,24},{20,28},{24,16},{28,20},{1,9},{5... | collective-permute-start | bytes 12296 | tf_op jit(solution)/shard_map/ppermute | solution.py:25
  24.9 3.1 %collective-permute-start.3 = (f32[2,512]{1,0:T(2,128)S(1)}, f32[2,512]{1,0:T(2,128)S(1)}, u32[]{:S(2)}, u32[]{:S(2)}) collective-permute-start(f32[2,512]{1,0:T(2,128)S(1)} %pad_maximum_fusion.1), channel_id=1, source_target_pairs={{0,16},{4,20},{8,24},{12,28},{16,0},{20,4},{24,8},{28,12},{1,17},{... | collective-permute-start | bytes 12296 | tf_op jit(solution)/shard_map/ppermute | solution.py:25
  30.2 2.7 %finish_branch.1 = (bf16[2,128,512]{2,1,0:T(8,128)(2,1)}, bf16[2,128,512]{2,1,0:T(8,128)(2,1)}) custom-call(s32[2]{0:T(128)} %pad_add_fusion.place, f32[1,512]{1,0:T(1,128)} %broadcast_select_fusion.6.entering, f32[4,512,128]{2,1,0:T(8,128)} %get-tuple-element.38.local, f32[4,512,128]{2,1,0:T(8,128)} %get-tuple-element.39.running, bf16[512,512]{1,0:T(8,128)(2,1)} %gate.1), custom_call_target="tpu_custom_call" | custom-call | flops 5242880 | bytes 3145728 | tf_op jit(solution)/shard_map/finish_branch/pallas_call | solution.py:208
  36.8 2.1 %fusion.1 = f32[128,2048]{1,0:T(8,128)S(1)} fusion(bf16[512,2048]{1,0:T(8,128)(2,1)} %param.23, bf16[2,128,512]{2,1,0:T(8,128)(2,1)} %get-tuple-element.40), kind=kOutput, calls=%fused_computation.5 | convolution fusion | flops 268435456 | bytes 3276800 | tf_op jit(solution)/shard_map/dot_general | solution.py:496
  39.5 2.9 %fusion = bf16[128,2048]{1,0:T(8,128)(2,1)} fusion(f32[128,2048]{1,0:T(8,128)S(1)} %fusion.1, bf16[512,2048]{1,0:T(8,128)(2,1)} %collective-permute-done.5, bf16[2,128,512]{2,1,0:T(8,128)(2,1)S(1)} %copy-done.17), kind=kOutput, calls=%fused_computation.2 | convolution fusion | flops 268959744 | bytes 3801088 | tf_op jit(solution)/shard_map/dot_general | solution.py:497
  42.4 7.9 %collective-permute-done.17.refs_14_.refs_10_ = bf16[512,512]{1,0:T(8,128)(2,1)S(1)} collective-permute-done((bf16[512,512]{1,0:T(8,128)(2,1)}, bf16[512,512]{1,0:T(8,128)(2,1)S(1)}, u32[]{:S(2)}, u32[]{:S(2)}) %collective-permute-start.17) | collective-permute-done | bytes 524320 | tf_op jit(solution)/shard_map/ppermute | solution.py:34
  54.8 6.8 %collective-permute-done.18.refs_15_.refs_11_ = bf16[512,512]{1,0:T(8,128)(2,1)S(1)} collective-permute-done((bf16[512,512]{1,0:T(8,128)(2,1)}, bf16[512,512]{1,0:T(8,128)(2,1)S(1)}, u32[]{:S(2)}, u32[]{:S(2)}) %collective-permute-start.18) | collective-permute-done | bytes 524320 | tf_op jit(solution)/shard_map/ppermute | solution.py:34
  61.6 10.5 %collective-permute-done.6.refs_0_ = bf16[128,2048]{1,0:T(8,128)(2,1)} collective-permute-done((bf16[128,2048]{1,0:T(8,128)(2,1)}, bf16[128,2048]{1,0:T(8,128)(2,1)}, u32[]{:S(2)}, u32[]{:S(2)}) %collective-permute-start.6) | collective-permute-done | bytes 524320 | tf_op jit(solution)/shard_map/ppermute | solution.py:34
  72.1 2.1 %fusion.3 = f32[128,2048]{1,0:T(8,128)S(1)} fusion(bf16[512,2048]{1,0:T(8,128)(2,1)} %param.23, bf16[2,128,512]{2,1,0:T(8,128)(2,1)S(1)} %copy-done.15), kind=kOutput, calls=%fused_computation.7 | convolution fusion | flops 268435456 | bytes 3276800 | tf_op jit(solution)/shard_map/dot_general | solution.py:496
  74.2 2.2 %convolution_add_fusion.1.own = f32[128,2048]{1,0:T(8,128)S(1)} fusion(f32[128,2048]{1,0:T(8,128)S(1)} %fusion.3, bf16[512,2048]{1,0:T(8,128)(2,1)} %collective-permute-done.5, bf16[2,128,512]{2,1,0:T(8,128)(2,1)S(1)} %copy-done.18), kind=kOutput, calls=%fused_computation.1 | convolution fusion | flops 268697600 | bytes 4325376 | tf_op jit(solution)/shard_map/dot_general | solution.py:497
  76.5 2.1 %send_rows.1 = (bf16[128,2048]{1,0:T(8,128)(2,1)S(1)}, bf16[48,2048]{1,0:T(8,128)(2,1)S(1)}, bf16[48,2048]{1,0:T(8,128)(2,1)S(1)}, bf16[48,2048]{1,0:T(8,128)(2,...) custom-call(bf16[128,2048]{1,0:T(8,128)(2,1)S(1)} %copy-done.4, ...), custom_call_target="tpu_custom_call" | custom-call | flops 201326592 | bytes 2097152 | tf_op jit(solution)/shard_map/send_rows/pallas_call | solution.py:255
  79.3 3.9 %collective-permute-start.36 = (bf16[48,2048]{1,0:T(8,128)(2,1)S(1)}, bf16[48,2048]{1,0:T(8,128)(2,1)S(1)}, u32[]{:S(2)}, u32[]{:S(2)}) collective-permute-start(bf16[48,2048]{1,0:T(8,128)(2,1)S(1)} %get-tuple-element.63), channel_id=1, source_target_pairs={{0,24},{4,28},{8,16},{12,20},{16,8},{20,12},{24,0},{28,4},{1,25},{... | collective-permute-start | bytes 589832 | tf_op jit(solution)/shard_map/ppermute | solution.py:25
  84.3 2.8 %collective-permute-start.29 = (bf16[48,2048]{1,0:T(8,128)(2,1)S(1)}, bf16[48,2048]{1,0:T(8,128)(2,1)S(1)}, u32[]{:S(2)}, u32[]{:S(2)}) collective-permute-start(bf16[48,2048]{1,0:T(8,128)(2,1)S(1)} %get-tuple-element.58), channel_id=1, source_target_pairs={{0,20},{4,16},{8,28},{12,24},{16,4},{20,0},{24,12},{28,8},{1,21},{... | collective-permute-start | bytes 589832 | tf_op jit(solution)/shard_map/ppermute | solution.py:25
  90.6 3.1 %collective-permute-done.37.refs_1_ = bf16[48,2048]{1,0:T(8,128)(2,1)S(1)} collective-permute-done((bf16[48,2048]{1,0:T(8,128)(2,1)S(1)}, bf16[48,2048]{1,0:T(8,128)(2,1)S(1)}, u32[]{:S(2)}, u32[]{:S(2)}) %collective-permute-start.37) | collective-permute-done | bytes 196640 | tf_op jit(solution)/shard_map/ppermute | solution.py:25
  96.3 17.4 %collective-permute-done.28.refs_0_ = bf16[48,2048]{1,0:T(8,128)(2,1)S(1)} collective-permute-done((bf16[48,2048]{1,0:T(8,128)(2,1)S(1)}, bf16[48,2048]{1,0:T(8,128)(2,1)S(1)}, u32[]{:S(2)}, u32[]{:S(2)}) %collective-permute-start.28) | collective-permute-done | bytes 196640 | tf_op jit(solution)/shard_map/ppermute | solution.py:25
  113.7 3.9 %collective-permute-done.29.refs_1_ = bf16[48,2048]{1,0:T(8,128)(2,1)S(1)} collective-permute-done((bf16[48,2048]{1,0:T(8,128)(2,1)S(1)}, bf16[48,2048]{1,0:T(8,128)(2,1)S(1)}, u32[]{:S(2)}, u32[]{:S(2)}) %collective-permute-start.29) | collective-permute-done | bytes 196640 | tf_op jit(solution)/shard_map/ppermute | solution.py:25
  119.6 5.7 %expert_rows.5 = (f32[48,2048]{1,0:T(8,128)S(1)}, f32[48,2048]{1,0:T(8,128)S(1)}, bf16[48,2048]{1,0:T(8,128)(2,1)S(1)}, bf16[48,2048]{1,0:T(8,128)(2,1)S(1)}) custom-call(s32[2]{0:T(128)S(1)} %copy-done.13, bf16[48,2048]{1,0:T(8,128)(2,1)S(1)} %collective-permute-done.36.refs_0_, bf16[48,2048]{1,0:T(8,128)(2,1)S(1)} %collective-permute-done.37.refs_1_, ...), custom_call_target="tpu_custom_call" | custom-call | flops 2415919104 | bytes 12582912 | tf_op jit(solution)/shard_map/expert_rows/pallas_call | solution.py:315
  131.0 5.7 %expert_rows.4 = (f32[48,2048]{1,0:T(8,128)S(1)}, f32[48,2048]{1,0:T(8,128)S(1)}, bf16[48,2048]{1,0:T(8,128)(2,1)S(1)}, bf16[48,2048]{1,0:T(8,128)(2,1)S(1)}) custom-call(s32[2]{0:T(128)S(1)} %copy-done.13, bf16[48,2048]{1,0:T(8,128)(2,1)S(1)} %collective-permute-done.28.refs_0_, bf16[48,2048]{1,0:T(8,128)(2,1)S(1)} %collective-permute-done.29.refs_1_, ...), custom_call_target="tpu_custom_call" | custom-call | flops 2415919104 | bytes 12582912 | tf_op jit(solution)/shard_map/expert_rows/pallas_call | solution.py:315
  139.3 2.7 %collective-permute-done.12.refs_6_ = bf16[48,2048]{1,0:T(8,128)(2,1)S(1)} collective-permute-done((bf16[48,2048]{1,0:T(8,128)(2,1)S(1)}, bf16[48,2048]{1,0:T(8,128)(2,1)S(1)}, u32[]{:S(2)}, u32[]{:S(2)}) %collective-permute-start.12) | collective-permute-done | bytes 196640 | tf_op jit(solution)/shard_map/ppermute | solution.py:34
  143.5 2.7 %collective-permute-done.13.refs_7_ = bf16[48,2048]{1,0:T(8,128)(2,1)S(1)} collective-permute-done((bf16[48,2048]{1,0:T(8,128)(2,1)S(1)}, bf16[48,2048]{1,0:T(8,128)(2,1)S(1)}, u32[]{:S(2)}, u32[]{:S(2)}) %collective-permute-start.13) | collective-permute-done | bytes 196640 | tf_op jit(solution)/shard_map/ppermute | solution.py:34
  146.2 8.1 %expert_rows.3 = (f32[48,2048]{1,0:T(8,128)S(1)}, f32[48,2048]{1,0:T(8,128)S(1)}, f32[48,2048]{1,0:T(8,128)S(1)}, f32[48,2048]{1,0:T(8,128)S(1)}, bf16[48,2048]{...) custom-call(s32[2]{0:T(128)S(1)} %copy-done.13, ...), custom_call_target="tpu_custom_call" | custom-call | flops 4831838208 | bytes 12582912 | tf_op jit(solution)/shard_map/expert_rows/pallas_call | solution.py:315
  160.4 2.7 %collective-permute-done.32.refs_0_ = bf16[48,2048]{1,0:T(8,128)(2,1)S(1)} collective-permute-done((bf16[48,2048]{1,0:T(8,128)(2,1)S(1)}, bf16[48,2048]{1,0:T(8,128)(2,1)S(1)}, u32[]{:S(2)}, u32[]{:S(2)}) %collective-permute-start.32) | collective-permute-done | bytes 196640 | tf_op jit(solution)/shard_map/ppermute | solution.py:34
  163.0 3.3 %collective-permute-start.43 = (bf16[48,2048]{1,0:T(8,128)(2,1)S(1)}, bf16[48,2048]{1,0:T(8,128)(2,1)S(1)}, u32[]{:S(2)}, u32[]{:S(2)}) collective-permute-start(bf16[48,2048]{1,0:T(8,128)(2,1)S(1)} %sum_rows.15), channel_id=1, source_target_pairs={{0,28},{4,24},{8,20},{12,16},{16,12},{20,8},{24,4},{28,0},{1,29},{... | collective-permute-start | bytes 589832 | tf_op jit(solution)/shard_map/ppermute | solution.py:25
  167.3 2.5 %collective-permute-start.41 = (bf16[48,2048]{1,0:T(8,128)(2,1)S(1)}, bf16[48,2048]{1,0:T(8,128)(2,1)S(1)}, u32[]{:S(2)}, u32[]{:S(2)}) collective-permute-start(bf16[48,2048]{1,0:T(8,128)(2,1)S(1)} %sum_rows.14), channel_id=1, source_target_pairs={{0,24},{4,28},{8,16},{12,20},{16,8},{20,12},{24,0},{28,4},{1,25},{... | collective-permute-start | bytes 589832 | tf_op jit(solution)/shard_map/ppermute | solution.py:25
  171.5 3.7 %collective-permute-start.35 = (bf16[48,2048]{1,0:T(8,128)(2,1)S(1)}, bf16[48,2048]{1,0:T(8,128)(2,1)S(1)}, u32[]{:S(2)}, u32[]{:S(2)}) collective-permute-start(bf16[48,2048]{1,0:T(8,128)(2,1)S(1)} %sum_rows.13), channel_id=1, source_target_pairs={{0,20},{4,16},{8,28},{12,24},{16,4},{20,0},{24,12},{28,8},{1,21},{... | collective-permute-start | bytes 589832 | tf_op jit(solution)/shard_map/ppermute | solution.py:25
  175.7 3.6 %collective-permute-start.33 = (bf16[48,2048]{1,0:T(8,128)(2,1)S(1)}, bf16[48,2048]{1,0:T(8,128)(2,1)}, u32[]{:S(2)}, u32[]{:S(2)}) collective-permute-start(bf16[48,2048]{1,0:T(8,128)(2,1)S(1)} %sum_rows.12), channel_id=1, source_target_pairs={{0,16},{4,20},{8,24},{12,28},{16,0},{20,4},{24,8},{28,12},{1,17},{... | collective-permute-start | bytes 589832 | tf_op jit(solution)/shard_map/ppermute | solution.py:25
  181.4 8.1 %collective-permute-start.25 = (bf16[48,2048]{1,0:T(8,128)(2,1)S(1)}, bf16[48,2048]{1,0:T(8,128)(2,1)S(1)}, u32[]{:S(2)}, u32[]{:S(2)}) collective-permute-start(bf16[48,2048]{1,0:T(8,128)(2,1)S(1)} %sum_rows.10), channel_id=1, source_target_pairs={{0,8},{4,12},{8,0},{12,4},{16,24},{20,28},{24,16},{28,20},{1,9},{5... | collective-permute-start | bytes 589832 | tf_op jit(solution)/shard_map/ppermute | solution.py:25
  191.6 5.3 %collective-permute-done.35.refs_5_ = bf16[48,2048]{1,0:T(8,128)(2,1)S(1)} collective-permute-done((bf16[48,2048]{1,0:T(8,128)(2,1)S(1)}, bf16[48,2048]{1,0:T(8,128)(2,1)S(1)}, u32[]{:S(2)}, u32[]{:S(2)}) %collective-permute-start.35) | collective-permute-done | bytes 196640 | tf_op jit(solution)/shard_map/ppermute | solution.py:25
  202.7 2.6 %blend_rows.1 = bf16[128,2048]{1,0:T(8,128)(2,1)} custom-call(bf16[128,2048]{1,0:T(8,128)(2,1)S(1)} %copy-done.6, bf16[256,384]{1,0:T(8,128)(2,1)S(1)} %mix_weights.1.mix, bf16[48,2048]{1,0:T(8,128)(2,1)S(1)} %sum_rows.8.refs_0_, bf16[48,2048]{1,0:T(8,128)(2,1)} %collective-permute-done.23.refs_1_, bf16[48,2048]{1,0:T(8,128)(2,1)S(1)} %collective-permute-done.25.refs_2_, ...), custom_call_target="tpu_custom_call" | custom-call | flops 402653184 | bytes 2621440 | tf_op jit(solution)/shard_map/blend_rows/pallas_call | solution.py:397
  (139 shorter events, 57.2 us)
Async XLA Ops:
  0.0 38.9 %collective-permute-start.5 = (bf16[512,2048]{1,0:T(8,128)(2,1)}, bf16[512,2048]{1,0:T(8,128)(2,1)}, u32[]{:S(2)}, u32[]{:S(2)}) collective-permute-start(bf16[512,2048]{1,0:T(8,128)(2,1)} %param.23), channel_id=1, source_target_pairs={{0,1},{1,0},{2,3},{3,2},{4,5},{5,4},{6,7},{7,6},{8,9},{9,8},{10,11... | collective-permute-start | bytes 6291464 | tf_op jit(solution)/shard_map/ppermute | solution.py:29
  32.9 50.6 %collective-permute-start.16 = (bf16[2048,512]{1,0:T(8,128)(2,1)S(1)}, bf16[2048,512]{1,0:T(8,128)(2,1)}, u32[]{:S(2)}, u32[]{:S(2)}) collective-permute-start(bf16[2048,512]{1,0:T(8,128)(2,1)S(1)} %bitcast.33), channel_id=1, source_target_pairs={{0,1},{1,0},{2,3},{3,2},{4,5},{5,4},{6,7},{7,6},{8,9},{9,8},{10,11... | collective-permute-start | bytes 6291464 | tf_op jit(solution)/shard_map/ppermute | solution.py:29
  33.4 50.9 %collective-permute-start.14 = (bf16[2048,512]{1,0:T(8,128)(2,1)}, bf16[2048,512]{1,0:T(8,128)(2,1)}, u32[]{:S(2)}, u32[]{:S(2)}) collective-permute-start(bf16[2048,512]{1,0:T(8,128)(2,1)} %bitcast.37), channel_id=1, source_target_pairs={{0,1},{1,0},{2,3},{3,2},{4,5},{5,4},{6,7},{7,6},{8,9},{9,8},{10,11... | collective-permute-start | bytes 6291464 | tf_op jit(solution)/shard_map/ppermute | solution.py:29
  33.4 61.9 %collective-permute-start.15 = (bf16[2048,512]{1,0:T(8,128)(2,1)}, bf16[2048,512]{1,0:T(8,128)(2,1)}, u32[]{:S(2)}, u32[]{:S(2)}) collective-permute-start(bf16[2048,512]{1,0:T(8,128)(2,1)} %bitcast.41), channel_id=1, source_target_pairs={{0,1},{1,0},{2,3},{3,2},{4,5},{5,4},{6,7},{7,6},{8,9},{9,8},{10,11... | collective-permute-start | bytes 6291464 | tf_op jit(solution)/shard_map/ppermute | solution.py:29
  35.3 15.0 %collective-permute-start.17 = (bf16[512,512]{1,0:T(8,128)(2,1)}, bf16[512,512]{1,0:T(8,128)(2,1)S(1)}, u32[]{:S(2)}, u32[]{:S(2)}) collective-permute-start(bf16[512,512]{1,0:T(8,128)(2,1)} %get-tuple-element.47), channel_id=1, source_target_pairs={{0,2},{1,3},{2,0},{3,1},{4,6},{5,7},{6,4},{7,5},{8,10},{9,11},{10,... | collective-permute-start | bytes 1572872 | tf_op jit(solution)/shard_map/ppermute | solution.py:34
  39.0 22.6 %collective-permute-start.18 = (bf16[512,512]{1,0:T(8,128)(2,1)}, bf16[512,512]{1,0:T(8,128)(2,1)S(1)}, u32[]{:S(2)}, u32[]{:S(2)}) collective-permute-start(bf16[512,512]{1,0:T(8,128)(2,1)} %get-tuple-element.48), channel_id=1, source_target_pairs={{0,2},{1,3},{2,0},{3,1},{4,6},{5,7},{6,4},{7,5},{8,10},{9,11},{10,... | collective-permute-start | bytes 1572872 | tf_op jit(solution)/shard_map/ppermute | solution.py:34
  50.3 21.7 %collective-permute-start.6 = (bf16[128,2048]{1,0:T(8,128)(2,1)}, bf16[128,2048]{1,0:T(8,128)(2,1)}, u32[]{:S(2)}, u32[]{:S(2)}) collective-permute-start(bf16[128,2048]{1,0:T(8,128)(2,1)} %fusion), channel_id=1, source_target_pairs={{0,2},{1,3},{2,0},{3,1},{4,6},{5,7},{6,4},{7,5},{8,10},{9,11},{10,... | collective-permute-start | bytes 1572872 | tf_op jit(solution)/shard_map/ppermute | solution.py:34
  61.5 17.8 %collective-permute-start.19 = (bf16[512,512]{1,0:T(8,128)(2,1)S(1)}, bf16[512,512]{1,0:T(8,128)(2,1)S(1)}, u32[]{:S(2)}, u32[]{:S(2)}) collective-permute-start(bf16[512,512]{1,0:T(8,128)(2,1)S(1)} %collective-permute-done.17.refs_14_.refs_10_), channel_id=1, source_target_pairs={{0,1},{1,0},{2,3},{3,2},{4,5},{5,4},{6,7},{7,6},{8,9},{9,8},{10,11... | collective-permute-start | bytes 1572872 | tf_op jit(solution)/shard_map/ppermute | solution.py:29
  83.5 30.2 %collective-permute-start.28 = (bf16[48,2048]{1,0:T(8,128)(2,1)S(1)}, bf16[48,2048]{1,0:T(8,128)(2,1)S(1)}, u32[]{:S(2)}, u32[]{:S(2)}) collective-permute-start(bf16[48,2048]{1,0:T(8,128)(2,1)S(1)} %get-tuple-element.57), channel_id=1, source_target_pairs={{0,16},{4,20},{8,24},{12,28},{16,0},{20,4},{24,8},{28,12},{1,17},{... | collective-permute-start | bytes 589832 | tf_op jit(solution)/shard_map/ppermute | solution.py:25
  84.3 33.3 %collective-permute-start.29 = (bf16[48,2048]{1,0:T(8,128)(2,1)S(1)}, bf16[48,2048]{1,0:T(8,128)(2,1)S(1)}, u32[]{:S(2)}, u32[]{:S(2)}) collective-permute-start(bf16[48,2048]{1,0:T(8,128)(2,1)S(1)} %get-tuple-element.58), channel_id=1, source_target_pairs={{0,20},{4,16},{8,28},{12,24},{16,4},{20,0},{24,12},{28,8},{1,21},{... | collective-permute-start | bytes 589832 | tf_op jit(solution)/shard_map/ppermute | solution.py:25
  89.1 28.5 %collective-permute-start.38 = (bf16[48,2048]{1,0:T(8,128)(2,1)S(1)}, bf16[48,2048]{1,0:T(8,128)(2,1)S(1)}, u32[]{:S(2)}, u32[]{:S(2)}) collective-permute-start(bf16[48,2048]{1,0:T(8,128)(2,1)S(1)} %collective-permute-done.36.refs_0_), channel_id=1, source_target_pairs={{0,2},{1,3},{2,0},{3,1},{4,6},{5,7},{6,4},{7,5},{8,10},{9,11},{10,... | collective-permute-start | bytes 589832 | tf_op jit(solution)/shard_map/ppermute | solution.py:34
  93.8 25.4 %collective-permute-start.39 = (bf16[48,2048]{1,0:T(8,128)(2,1)S(1)}, bf16[48,2048]{1,0:T(8,128)(2,1)S(1)}, u32[]{:S(2)}, u32[]{:S(2)}) collective-permute-start(bf16[48,2048]{1,0:T(8,128)(2,1)S(1)} %collective-permute-done.37.refs_1_), channel_id=1, source_target_pairs={{0,2},{1,3},{2,0},{3,1},{4,6},{5,7},{6,4},{7,5},{8,10},{9,11},{10,... | collective-permute-start | bytes 589832 | tf_op jit(solution)/shard_map/ppermute | solution.py:34
  95.3 30.0 %collective-permute-start.7 = (bf16[48,2048]{1,0:T(8,128)(2,1)S(1)}, bf16[48,2048]{1,0:T(8,128)(2,1)S(1)}, u32[]{:S(2)}, u32[]{:S(2)}) collective-permute-start(bf16[48,2048]{1,0:T(8,128)(2,1)S(1)} %get-tuple-element.44), channel_id=1, source_target_pairs={{0,4},{4,0},{8,12},{12,8},{16,20},{20,16},{24,28},{28,24},{1,5},{5... | collective-permute-start | bytes 589832 | tf_op jit(solution)/shard_map/ppermute | solution.py:25
  113.7 13.2 %collective-permute-start.8 = (bf16[48,2048]{1,0:T(8,128)(2,1)S(1)}, bf16[48,2048]{1,0:T(8,128)(2,1)S(1)}, u32[]{:S(2)}, u32[]{:S(2)}) collective-permute-start(bf16[48,2048]{1,0:T(8,128)(2,1)S(1)} %get-tuple-element.45), channel_id=1, source_target_pairs={{0,8},{4,12},{8,0},{12,4},{16,24},{20,28},{24,16},{28,20},{1,9},{5... | collective-permute-start | bytes 589832 | tf_op jit(solution)/shard_map/ppermute | solution.py:25
  117.6 11.4 %collective-permute-start.30 = (bf16[48,2048]{1,0:T(8,128)(2,1)S(1)}, bf16[48,2048]{1,0:T(8,128)(2,1)S(1)}, u32[]{:S(2)}, u32[]{:S(2)}) collective-permute-start(bf16[48,2048]{1,0:T(8,128)(2,1)S(1)} %collective-permute-done.28.refs_0_), channel_id=1, source_target_pairs={{0,2},{1,3},{2,0},{3,1},{4,6},{5,7},{6,4},{7,5},{8,10},{9,11},{10,... | collective-permute-start | bytes 589832 | tf_op jit(solution)/shard_map/ppermute | solution.py:34
  127.5 14.5 %collective-permute-start.12 = (bf16[48,2048]{1,0:T(8,128)(2,1)S(1)}, bf16[48,2048]{1,0:T(8,128)(2,1)S(1)}, u32[]{:S(2)}, u32[]{:S(2)}) collective-permute-start(bf16[48,2048]{1,0:T(8,128)(2,1)S(1)} %collective-permute-done.8.refs_2_), channel_id=1, source_target_pairs={{0,2},{1,3},{2,0},{3,1},{4,6},{5,7},{6,4},{7,5},{8,10},{9,11},{10,... | collective-permute-start | bytes 589832 | tf_op jit(solution)/shard_map/ppermute | solution.py:34
  129.0 17.2 %collective-permute-start.13 = (bf16[48,2048]{1,0:T(8,128)(2,1)S(1)}, bf16[48,2048]{1,0:T(8,128)(2,1)S(1)}, u32[]{:S(2)}, u32[]{:S(2)}) collective-permute-start(bf16[48,2048]{1,0:T(8,128)(2,1)S(1)} %collective-permute-done.9.refs_3_), channel_id=1, source_target_pairs={{0,2},{1,3},{2,0},{3,1},{4,6},{5,7},{6,4},{7,5},{8,10},{9,11},{10,... | collective-permute-start | bytes 589832 | tf_op jit(solution)/shard_map/ppermute | solution.py:34
  129.5 26.4 %collective-permute-start.42 = (bf16[48,2048]{1,0:T(8,128)(2,1)S(1)}, bf16[48,2048]{1,0:T(8,128)(2,1)S(1)}, u32[]{:S(2)}, u32[]{:S(2)}) collective-permute-start(bf16[48,2048]{1,0:T(8,128)(2,1)S(1)} %get-tuple-element.68), channel_id=1, source_target_pairs={{0,2},{1,3},{2,0},{3,1},{4,6},{5,7},{6,4},{7,5},{8,10},{9,11},{10,... | collective-permute-start | bytes 589832 | tf_op jit(solution)/shard_map/ppermute | solution.py:34
  136.7 19.7 %collective-permute-start.40 = (bf16[48,2048]{1,0:T(8,128)(2,1)S(1)}, bf16[48,2048]{1,0:T(8,128)(2,1)S(1)}, u32[]{:S(2)}, u32[]{:S(2)}) collective-permute-start(bf16[48,2048]{1,0:T(8,128)(2,1)S(1)} %get-tuple-element.66), channel_id=1, source_target_pairs={{0,2},{1,3},{2,0},{3,1},{4,6},{5,7},{6,4},{7,5},{8,10},{9,11},{10,... | collective-permute-start | bytes 589832 | tf_op jit(solution)/shard_map/ppermute | solution.py:34
  137.8 21.1 %collective-permute-start.34 = (bf16[48,2048]{1,0:T(8,128)(2,1)S(1)}, bf16[48,2048]{1,0:T(8,128)(2,1)S(1)}, u32[]{:S(2)}, u32[]{:S(2)}) collective-permute-start(bf16[48,2048]{1,0:T(8,128)(2,1)S(1)} %get-tuple-element.62), channel_id=1, source_target_pairs={{0,2},{1,3},{2,0},{3,1},{4,6},{5,7},{6,4},{7,5},{8,10},{9,11},{10,... | collective-permute-start | bytes 589832 | tf_op jit(solution)/shard_map/ppermute | solution.py:34
  142.0 21.1 %collective-permute-start.32 = (bf16[48,2048]{1,0:T(8,128)(2,1)S(1)}, bf16[48,2048]{1,0:T(8,128)(2,1)S(1)}, u32[]{:S(2)}, u32[]{:S(2)}) collective-permute-start(bf16[48,2048]{1,0:T(8,128)(2,1)S(1)} %get-tuple-element.60), channel_id=1, source_target_pairs={{0,2},{1,3},{2,0},{3,1},{4,6},{5,7},{6,4},{7,5},{8,10},{9,11},{10,... | collective-permute-start | bytes 589832 | tf_op jit(solution)/shard_map/ppermute | solution.py:34
  154.4 12.9 %collective-permute-start.26 = (bf16[48,2048]{1,0:T(8,128)(2,1)S(1)}, bf16[48,2048]{1,0:T(8,128)(2,1)S(1)}, u32[]{:S(2)}, u32[]{:S(2)}) collective-permute-start(bf16[48,2048]{1,0:T(8,128)(2,1)S(1)} %get-tuple-element.56), channel_id=1, source_target_pairs={{0,2},{1,3},{2,0},{3,1},{4,6},{5,7},{6,4},{7,5},{8,10},{9,11},{10,... | collective-permute-start | bytes 589832 | tf_op jit(solution)/shard_map/ppermute | solution.py:34
  155.9 15.5 %collective-permute-start.24 = (bf16[48,2048]{1,0:T(8,128)(2,1)S(1)}, bf16[48,2048]{1,0:T(8,128)(2,1)S(1)}, u32[]{:S(2)}, u32[]{:S(2)}) collective-permute-start(bf16[48,2048]{1,0:T(8,128)(2,1)S(1)} %get-tuple-element.54), channel_id=1, source_target_pairs={{0,2},{1,3},{2,0},{3,1},{4,6},{5,7},{6,4},{7,5},{8,10},{9,11},{10,... | collective-permute-start | bytes 589832 | tf_op jit(solution)/shard_map/ppermute | solution.py:34
  156.5 19.2 %collective-permute-start.22 = (bf16[48,2048]{1,0:T(8,128)(2,1)S(1)}, bf16[48,2048]{1,0:T(8,128)(2,1)S(1)}, u32[]{:S(2)}, u32[]{:S(2)}) collective-permute-start(bf16[48,2048]{1,0:T(8,128)(2,1)S(1)} %get-tuple-element.52), channel_id=1, source_target_pairs={{0,2},{1,3},{2,0},{3,1},{4,6},{5,7},{6,4},{7,5},{8,10},{9,11},{10,... | collective-permute-start | bytes 589832 | tf_op jit(solution)/shard_map/ppermute | solution.py:34
  158.8 20.5 %collective-permute-start.21 = (bf16[48,2048]{1,0:T(8,128)(2,1)S(1)}, bf16[48,2048]{1,0:T(8,128)(2,1)S(1)}, u32[]{:S(2)}, u32[]{:S(2)}) collective-permute-start(bf16[48,2048]{1,0:T(8,128)(2,1)S(1)} %get-tuple-element.50), channel_id=1, source_target_pairs={{0,2},{1,3},{2,0},{3,1},{4,6},{5,7},{6,4},{7,5},{8,10},{9,11},{10,... | collective-permute-start | bytes 589832 | tf_op jit(solution)/shard_map/ppermute | solution.py:34
  163.0 18.3 %collective-permute-start.43 = (bf16[48,2048]{1,0:T(8,128)(2,1)S(1)}, bf16[48,2048]{1,0:T(8,128)(2,1)S(1)}, u32[]{:S(2)}, u32[]{:S(2)}) collective-permute-start(bf16[48,2048]{1,0:T(8,128)(2,1)S(1)} %sum_rows.15), channel_id=1, source_target_pairs={{0,28},{4,24},{8,20},{12,16},{16,12},{20,8},{24,4},{28,0},{1,29},{... | collective-permute-start | bytes 589832 | tf_op jit(solution)/shard_map/ppermute | solution.py:25
  167.3 22.2 %collective-permute-start.41 = (bf16[48,2048]{1,0:T(8,128)(2,1)S(1)}, bf16[48,2048]{1,0:T(8,128)(2,1)S(1)}, u32[]{:S(2)}, u32[]{:S(2)}) collective-permute-start(bf16[48,2048]{1,0:T(8,128)(2,1)S(1)} %sum_rows.14), channel_id=1, source_target_pairs={{0,24},{4,28},{8,16},{12,20},{16,8},{20,12},{24,0},{28,4},{1,25},{... | collective-permute-start | bytes 589832 | tf_op jit(solution)/shard_map/ppermute | solution.py:25
  171.5 25.4 %collective-permute-start.35 = (bf16[48,2048]{1,0:T(8,128)(2,1)S(1)}, bf16[48,2048]{1,0:T(8,128)(2,1)S(1)}, u32[]{:S(2)}, u32[]{:S(2)}) collective-permute-start(bf16[48,2048]{1,0:T(8,128)(2,1)S(1)} %sum_rows.13), channel_id=1, source_target_pairs={{0,20},{4,16},{8,28},{12,24},{16,4},{20,0},{24,12},{28,8},{1,21},{... | collective-permute-start | bytes 589832 | tf_op jit(solution)/shard_map/ppermute | solution.py:25
  175.7 23.7 %collective-permute-start.33 = (bf16[48,2048]{1,0:T(8,128)(2,1)S(1)}, bf16[48,2048]{1,0:T(8,128)(2,1)}, u32[]{:S(2)}, u32[]{:S(2)}) collective-permute-start(bf16[48,2048]{1,0:T(8,128)(2,1)S(1)} %sum_rows.12), channel_id=1, source_target_pairs={{0,16},{4,20},{8,24},{12,28},{16,0},{20,4},{24,8},{28,12},{1,17},{... | collective-permute-start | bytes 589832 | tf_op jit(solution)/shard_map/ppermute | solution.py:25
  179.4 20.1 %collective-permute-start.27 = (bf16[48,2048]{1,0:T(8,128)(2,1)S(1)}, bf16[48,2048]{1,0:T(8,128)(2,1)}, u32[]{:S(2)}, u32[]{:S(2)}) collective-permute-start(bf16[48,2048]{1,0:T(8,128)(2,1)S(1)} %sum_rows.11), channel_id=1, source_target_pairs={{0,12},{4,8},{8,4},{12,0},{16,28},{20,24},{24,20},{28,16},{1,13},{... | collective-permute-start | bytes 589832 | tf_op jit(solution)/shard_map/ppermute | solution.py:25
  181.4 19.5 %collective-permute-start.25 = (bf16[48,2048]{1,0:T(8,128)(2,1)S(1)}, bf16[48,2048]{1,0:T(8,128)(2,1)S(1)}, u32[]{:S(2)}, u32[]{:S(2)}) collective-permute-start(bf16[48,2048]{1,0:T(8,128)(2,1)S(1)} %sum_rows.10), channel_id=1, source_target_pairs={{0,8},{4,12},{8,0},{12,4},{16,24},{20,28},{24,16},{28,20},{1,9},{5... | collective-permute-start | bytes 589832 | tf_op jit(solution)/shard_map/ppermute | solution.py:25
  189.5 11.4 %collective-permute-start.23 = (bf16[48,2048]{1,0:T(8,128)(2,1)S(1)}, bf16[48,2048]{1,0:T(8,128)(2,1)}, u32[]{:S(2)}, u32[]{:S(2)}) collective-permute-start(bf16[48,2048]{1,0:T(8,128)(2,1)S(1)} %sum_rows.9), channel_id=1, source_target_pairs={{0,4},{4,0},{8,12},{12,8},{16,20},{20,16},{24,28},{28,24},{1,5},{5... | collective-permute-start | bytes 589832 | tf_op jit(solution)/shard_map/ppermute | solution.py:25
  (33 other events, 440.7 us)

commit v2 on v1

--- a/solution.py
+++ b/solution.py
@@ -91,10 +91,10 @@
     log_decay = -RECURRENT_SCALE * recur_gate * jax.nn.softplus(-slope[...]) + boost[...]
     decay = jnp.exp(log_decay)
     twice = 2.0 * log_decay
-    series = 1.0 + twice * (1.0 / 9.0)
-    for n in range(8, 1, -1):
+    series = 1.0 + twice * (1.0 / 6.0)
+    for n in range(5, 1, -1):
         series = 1.0 + twice * (1.0 / n) * series
-    lost = jnp.where(twice > -0.35, -twice * series, 1.0 - decay * decay)
+    lost = jnp.where(twice > -0.1, -twice * series, 1.0 - decay * decay)
     drive = jnp.sqrt(lost) * (input_gate * smoothed.astype(jnp.float32))
     groups, width = decays.shape[0], decays.shape[2]
     for g in range(groups):

time: 206 us -> 205 us (level)
  no operation moved by 1% of the time
where the time goes in v2:
time: 205 us
  waiting for transfers between devices  78.6 us (38%)
  starting transfers between devices  70.3 us (34%)
  Pallas kernels  34.7 us (17%)
  matrix products  9.3 us (5%)
  local copies, waits for them, and re-layouts  7.92 us (4%)
  other arithmetic  3.7 us (2%)
    ppermute x17, starting transfers between devices, across(): lax.ppermute(block, 'sp', [(i, i ^ bits) for i in range(lax.axis_size('sp...  41.3 us
    ppermute x17, waiting for transfers between devices, across(): lax.ppermute(block, 'sp', [(i, i ^ bits) for i in range(lax.axis_size('sp...  40 us
    ppermute x19, waiting for transfers between devices, turned(): lax.ppermute(block, 'tp', [(i, (i + 2 * distance) % size) for i in range(...  37.4 us
    ppermute x19, starting transfers between devices, turned(): lax.ppermute(block, 'tp', [(i, (i + 2 * distance) % size) for i in range(...  23.1 us
    pallas_call x3, Pallas kernels, expert_rows(): pl.pallas_call(functools.partial(expert_kernel, groups=len(rows), outs=le...  19.5 us
    pallas_call x1, Pallas kernels, local_scan(): pl.pallas_call(scan_kernel, grid=(channels // lanes,), in_specs=[pl.Block...  7.32 us
    unnamed x44, local copies, waits for them, and re-layouts  5.9 us
    dot_general x2, matrix products, projected(): jnp.dot(taken[d], projection_far, preferred_element_type=jnp.float32)  5.13 us
  transfers between devices with their start and end apart: 44, of which 23 were waited for; matrix products, arithmetic and copies ran while one was open for 7% of the time, Pallas kernels for 16%

profile of v2, /device:TPU:0, one launch (start us, length us, event | category | flops | bytes accessed | tf_op | source)
XLA Modules:
  0.0 204.9 jit_solution(8520255444777366931)
XLA Ops:
  1.2 4.4 %collective-permute-start = (bf16[8,512]{1,0:T(8,128)(2,1)S(1)}, bf16[8,512]{1,0:T(8,128)(2,1)S(1)}, u32[]{:S(2)}, u32[]{:S(2)}) collective-permute-start(bf16[8,512]{1,0:T(8,128)(2,1)S(1)} %slice.43), channel_id=1, source_target_pairs={{0,4},{4,8},{8,12},{12,16},{16,20},{20,24},{24,28},{1,5},{5,9},{9,... | collective-permute-start | bytes 24584 | tf_op jit(solution)/shard_map/ppermute | solution.py:21
  7.5 7.3 %local_scan.1 = (f32[4,512,128]{2,1,0:T(8,128)}, f32[4,512,128]{2,1,0:T(8,128)}, f32[2,512]{1,0:T(2,128)}, bf16[512,512]{1,0:T(8,128)(2,1)}, bf16[512,512]{1,0:T(8,128)(2,1)}) custom-call(s32[2]{0:T(128)} %pad_add_fusion.place, bf16[8,512]{1,0:T(8,128)(2,1)} %copy-done.19, bf16[512,512]{1,0:T(8,128)(2,1)} %x.1, f32[4,512]{1,0:T(4,128)} %taps.1, ...), custom_call_target="tpu_custom_call" | custom-call | tf_op jit(solution)/shard_map/local_scan/pallas_call | solution.py:144
  14.9 2.4 %collective-permute-start.1 = (f32[2,512]{1,0:T(2,128)}, f32[2,512]{1,0:T(2,128)S(1)}, u32[]{:S(2)}, u32[]{:S(2)}) collective-permute-start(f32[2,512]{1,0:T(2,128)} %get-tuple-element.37), channel_id=1, source_target_pairs={{0,4},{4,0},{8,12},{12,8},{16,20},{20,16},{24,28},{28,24},{1,5},{5... | collective-permute-start | bytes 12296 | tf_op jit(solution)/shard_map/ppermute | solution.py:25
  19.8 3.1 %collective-permute-start.2 = (f32[2,512]{1,0:T(2,128)S(1)}, f32[2,512]{1,0:T(2,128)S(1)}, u32[]{:S(2)}, u32[]{:S(2)}) collective-permute-start(f32[2,512]{1,0:T(2,128)S(1)} %pad_maximum_fusion), channel_id=1, source_target_pairs={{0,8},{4,12},{8,0},{12,4},{16,24},{20,28},{24,16},{28,20},{1,9},{5... | collective-permute-start | bytes 12296 | tf_op jit(solution)/shard_map/ppermute | solution.py:25
  24.5 3.1 %collective-permute-start.3 = (f32[2,512]{1,0:T(2,128)S(1)}, f32[2,512]{1,0:T(2,128)S(1)}, u32[]{:S(2)}, u32[]{:S(2)}) collective-permute-start(f32[2,512]{1,0:T(2,128)S(1)} %pad_maximum_fusion.1), channel_id=1, source_target_pairs={{0,16},{4,20},{8,24},{12,28},{16,0},{20,4},{24,8},{28,12},{1,17},{... | collective-permute-start | bytes 12296 | tf_op jit(solution)/shard_map/ppermute | solution.py:25
  29.8 2.7 %finish_branch.1 = (bf16[2,128,512]{2,1,0:T(8,128)(2,1)}, bf16[2,128,512]{2,1,0:T(8,128)(2,1)}) custom-call(s32[2]{0:T(128)} %pad_add_fusion.place, f32[1,512]{1,0:T(1,128)} %broadcast_select_fusion.6.entering, f32[4,512,128]{2,1,0:T(8,128)} %get-tuple-element.38.local, f32[4,512,128]{2,1,0:T(8,128)} %get-tuple-element.39.running, bf16[512,512]{1,0:T(8,128)(2,1)} %gate.1), custom_call_target="tpu_custom_call" | custom-call | flops 5242880 | bytes 3145728 | tf_op jit(solution)/shard_map/finish_branch/pallas_call | solution.py:208
  36.4 2.1 %fusion.1 = f32[128,2048]{1,0:T(8,128)S(1)} fusion(bf16[512,2048]{1,0:T(8,128)(2,1)} %param.23, bf16[2,128,512]{2,1,0:T(8,128)(2,1)} %get-tuple-element.40), kind=kOutput, calls=%fused_computation.5 | convolution fusion | flops 268435456 | bytes 3276800 | tf_op jit(solution)/shard_map/dot_general | solution.py:496
  39.1 2.9 %fusion = bf16[128,2048]{1,0:T(8,128)(2,1)} fusion(f32[128,2048]{1,0:T(8,128)S(1)} %fusion.1, bf16[512,2048]{1,0:T(8,128)(2,1)} %collective-permute-done.5, bf16[2,128,512]{2,1,0:T(8,128)(2,1)S(1)} %copy-done.17), kind=kOutput, calls=%fused_computation.2 | convolution fusion | flops 268959744 | bytes 3801088 | tf_op jit(solution)/shard_map/dot_general | solution.py:497
  42.0 7.9 %collective-permute-done.17.refs_14_.refs_10_ = bf16[512,512]{1,0:T(8,128)(2,1)S(1)} collective-permute-done((bf16[512,512]{1,0:T(8,128)(2,1)}, bf16[512,512]{1,0:T(8,128)(2,1)S(1)}, u32[]{:S(2)}, u32[]{:S(2)}) %collective-permute-start.17) | collective-permute-done | bytes 524320 | tf_op jit(solution)/shard_map/ppermute | solution.py:34
  54.4 6.8 %collective-permute-done.18.refs_15_.refs_11_ = bf16[512,512]{1,0:T(8,128)(2,1)S(1)} collective-permute-done((bf16[512,512]{1,0:T(8,128)(2,1)}, bf16[512,512]{1,0:T(8,128)(2,1)S(1)}, u32[]{:S(2)}, u32[]{:S(2)}) %collective-permute-start.18) | collective-permute-done | bytes 524320 | tf_op jit(solution)/shard_map/ppermute | solution.py:34
  61.1 10.5 %collective-permute-done.6.refs_0_ = bf16[128,2048]{1,0:T(8,128)(2,1)} collective-permute-done((bf16[128,2048]{1,0:T(8,128)(2,1)}, bf16[128,2048]{1,0:T(8,128)(2,1)}, u32[]{:S(2)}, u32[]{:S(2)}) %collective-permute-start.6) | collective-permute-done | bytes 524320 | tf_op jit(solution)/shard_map/ppermute | solution.py:34
  71.7 2.1 %fusion.3 = f32[128,2048]{1,0:T(8,128)S(1)} fusion(bf16[512,2048]{1,0:T(8,128)(2,1)} %param.23, bf16[2,128,512]{2,1,0:T(8,128)(2,1)S(1)} %copy-done.15), kind=kOutput, calls=%fused_computation.7 | convolution fusion | flops 268435456 | bytes 3276800 | tf_op jit(solution)/shard_map/dot_general | solution.py:496
  73.8 2.2 %convolution_add_fusion.1.own = f32[128,2048]{1,0:T(8,128)S(1)} fusion(f32[128,2048]{1,0:T(8,128)S(1)} %fusion.3, bf16[512,2048]{1,0:T(8,128)(2,1)} %collective-permute-done.5, bf16[2,128,512]{2,1,0:T(8,128)(2,1)S(1)} %copy-done.18), kind=kOutput, calls=%fused_computation.1 | convolution fusion | flops 268697600 | bytes 4325376 | tf_op jit(solution)/shard_map/dot_general | solution.py:497
  76.0 2.1 %send_rows.1 = (bf16[128,2048]{1,0:T(8,128)(2,1)S(1)}, bf16[48,2048]{1,0:T(8,128)(2,1)S(1)}, bf16[48,2048]{1,0:T(8,128)(2,1)S(1)}, bf16[48,2048]{1,0:T(8,128)(2,...) custom-call(bf16[128,2048]{1,0:T(8,128)(2,1)S(1)} %copy-done.4, ...), custom_call_target="tpu_custom_call" | custom-call | flops 201326592 | bytes 2097152 | tf_op jit(solution)/shard_map/send_rows/pallas_call | solution.py:255
  78.9 3.9 %collective-permute-start.36 = (bf16[48,2048]{1,0:T(8,128)(2,1)S(1)}, bf16[48,2048]{1,0:T(8,128)(2,1)S(1)}, u32[]{:S(2)}, u32[]{:S(2)}) collective-permute-start(bf16[48,2048]{1,0:T(8,128)(2,1)S(1)} %get-tuple-element.63), channel_id=1, source_target_pairs={{0,24},{4,28},{8,16},{12,20},{16,8},{20,12},{24,0},{28,4},{1,25},{... | collective-permute-start | bytes 589832 | tf_op jit(solution)/shard_map/ppermute | solution.py:25
  83.9 2.9 %collective-permute-start.29 = (bf16[48,2048]{1,0:T(8,128)(2,1)S(1)}, bf16[48,2048]{1,0:T(8,128)(2,1)S(1)}, u32[]{:S(2)}, u32[]{:S(2)}) collective-permute-start(bf16[48,2048]{1,0:T(8,128)(2,1)S(1)} %get-tuple-element.58), channel_id=1, source_target_pairs={{0,20},{4,16},{8,28},{12,24},{16,4},{20,0},{24,12},{28,8},{1,21},{... | collective-permute-start | bytes 589832 | tf_op jit(solution)/shard_map/ppermute | solution.py:25
  90.2 3.2 %collective-permute-done.37.refs_1_ = bf16[48,2048]{1,0:T(8,128)(2,1)S(1)} collective-permute-done((bf16[48,2048]{1,0:T(8,128)(2,1)S(1)}, bf16[48,2048]{1,0:T(8,128)(2,1)S(1)}, u32[]{:S(2)}, u32[]{:S(2)}) %collective-permute-start.37) | collective-permute-done | bytes 196640 | tf_op jit(solution)/shard_map/ppermute | solution.py:25
  95.9 17.4 %collective-permute-done.28.refs_0_ = bf16[48,2048]{1,0:T(8,128)(2,1)S(1)} collective-permute-done((bf16[48,2048]{1,0:T(8,128)(2,1)S(1)}, bf16[48,2048]{1,0:T(8,128)(2,1)S(1)}, u32[]{:S(2)}, u32[]{:S(2)}) %collective-permute-start.28) | collective-permute-done | bytes 196640 | tf_op jit(solution)/shard_map/ppermute | solution.py:25
  113.3 3.9 %collective-permute-done.29.refs_1_ = bf16[48,2048]{1,0:T(8,128)(2,1)S(1)} collective-permute-done((bf16[48,2048]{1,0:T(8,128)(2,1)S(1)}, bf16[48,2048]{1,0:T(8,128)(2,1)S(1)}, u32[]{:S(2)}, u32[]{:S(2)}) %collective-permute-start.29) | collective-permute-done | bytes 196640 | tf_op jit(solution)/shard_map/ppermute | solution.py:25
  119.2 5.7 %expert_rows.5 = (f32[48,2048]{1,0:T(8,128)S(1)}, f32[48,2048]{1,0:T(8,128)S(1)}, bf16[48,2048]{1,0:T(8,128)(2,1)S(1)}, bf16[48,2048]{1,0:T(8,128)(2,1)S(1)}) custom-call(s32[2]{0:T(128)S(1)} %copy-done.13, bf16[48,2048]{1,0:T(8,128)(2,1)S(1)} %collective-permute-done.36.refs_0_, bf16[48,2048]{1,0:T(8,128)(2,1)S(1)} %collective-permute-done.37.refs_1_, ...), custom_call_target="tpu_custom_call" | custom-call | flops 2415919104 | bytes 12582912 | tf_op jit(solution)/shard_map/expert_rows/pallas_call | solution.py:315
  130.6 5.7 %expert_rows.4 = (f32[48,2048]{1,0:T(8,128)S(1)}, f32[48,2048]{1,0:T(8,128)S(1)}, bf16[48,2048]{1,0:T(8,128)(2,1)S(1)}, bf16[48,2048]{1,0:T(8,128)(2,1)S(1)}) custom-call(s32[2]{0:T(128)S(1)} %copy-done.13, bf16[48,2048]{1,0:T(8,128)(2,1)S(1)} %collective-permute-done.28.refs_0_, bf16[48,2048]{1,0:T(8,128)(2,1)S(1)} %collective-permute-done.29.refs_1_, ...), custom_call_target="tpu_custom_call" | custom-call | flops 2415919104 | bytes 12582912 | tf_op jit(solution)/shard_map/expert_rows/pallas_call | solution.py:315
  138.9 2.7 %collective-permute-done.12.refs_6_ = bf16[48,2048]{1,0:T(8,128)(2,1)S(1)} collective-permute-done((bf16[48,2048]{1,0:T(8,128)(2,1)S(1)}, bf16[48,2048]{1,0:T(8,128)(2,1)S(1)}, u32[]{:S(2)}, u32[]{:S(2)}) %collective-permute-start.12) | collective-permute-done | bytes 196640 | tf_op jit(solution)/shard_map/ppermute | solution.py:34
  143.1 2.7 %collective-permute-done.13.refs_7_ = bf16[48,2048]{1,0:T(8,128)(2,1)S(1)} collective-permute-done((bf16[48,2048]{1,0:T(8,128)(2,1)S(1)}, bf16[48,2048]{1,0:T(8,128)(2,1)S(1)}, u32[]{:S(2)}, u32[]{:S(2)}) %collective-permute-start.13) | collective-permute-done | bytes 196640 | tf_op jit(solution)/shard_map/ppermute | solution.py:34
  145.8 8.1 %expert_rows.3 = (f32[48,2048]{1,0:T(8,128)S(1)}, f32[48,2048]{1,0:T(8,128)S(1)}, f32[48,2048]{1,0:T(8,128)S(1)}, f32[48,2048]{1,0:T(8,128)S(1)}, bf16[48,2048]{...) custom-call(s32[2]{0:T(128)S(1)} %copy-done.13, ...), custom_call_target="tpu_custom_call" | custom-call | flops 4831838208 | bytes 12582912 | tf_op jit(solution)/shard_map/expert_rows/pallas_call | solution.py:315
  159.9 2.7 %collective-permute-done.32.refs_0_ = bf16[48,2048]{1,0:T(8,128)(2,1)S(1)} collective-permute-done((bf16[48,2048]{1,0:T(8,128)(2,1)S(1)}, bf16[48,2048]{1,0:T(8,128)(2,1)S(1)}, u32[]{:S(2)}, u32[]{:S(2)}) %collective-permute-start.32) | collective-permute-done | bytes 196640 | tf_op jit(solution)/shard_map/ppermute | solution.py:34
  162.6 3.3 %collective-permute-start.43 = (bf16[48,2048]{1,0:T(8,128)(2,1)S(1)}, bf16[48,2048]{1,0:T(8,128)(2,1)S(1)}, u32[]{:S(2)}, u32[]{:S(2)}) collective-permute-start(bf16[48,2048]{1,0:T(8,128)(2,1)S(1)} %sum_rows.15), channel_id=1, source_target_pairs={{0,28},{4,24},{8,20},{12,16},{16,12},{20,8},{24,4},{28,0},{1,29},{... | collective-permute-start | bytes 589832 | tf_op jit(solution)/shard_map/ppermute | solution.py:25
  166.9 2.5 %collective-permute-start.41 = (bf16[48,2048]{1,0:T(8,128)(2,1)S(1)}, bf16[48,2048]{1,0:T(8,128)(2,1)S(1)}, u32[]{:S(2)}, u32[]{:S(2)}) collective-permute-start(bf16[48,2048]{1,0:T(8,128)(2,1)S(1)} %sum_rows.14), channel_id=1, source_target_pairs={{0,24},{4,28},{8,16},{12,20},{16,8},{20,12},{24,0},{28,4},{1,25},{... | collective-permute-start | bytes 589832 | tf_op jit(solution)/shard_map/ppermute | solution.py:25
  171.1 3.7 %collective-permute-start.35 = (bf16[48,2048]{1,0:T(8,128)(2,1)S(1)}, bf16[48,2048]{1,0:T(8,128)(2,1)S(1)}, u32[]{:S(2)}, u32[]{:S(2)}) collective-permute-start(bf16[48,2048]{1,0:T(8,128)(2,1)S(1)} %sum_rows.13), channel_id=1, source_target_pairs={{0,20},{4,16},{8,28},{12,24},{16,4},{20,0},{24,12},{28,8},{1,21},{... | collective-permute-start | bytes 589832 | tf_op jit(solution)/shard_map/ppermute | solution.py:25
  175.3 3.6 %collective-permute-start.33 = (bf16[48,2048]{1,0:T(8,128)(2,1)S(1)}, bf16[48,2048]{1,0:T(8,128)(2,1)}, u32[]{:S(2)}, u32[]{:S(2)}) collective-permute-start(bf16[48,2048]{1,0:T(8,128)(2,1)S(1)} %sum_rows.12), channel_id=1, source_target_pairs={{0,16},{4,20},{8,24},{12,28},{16,0},{20,4},{24,8},{28,12},{1,17},{... | collective-permute-start | bytes 589832 | tf_op jit(solution)/shard_map/ppermute | solution.py:25
  181.0 8.0 %collective-permute-start.25 = (bf16[48,2048]{1,0:T(8,128)(2,1)S(1)}, bf16[48,2048]{1,0:T(8,128)(2,1)S(1)}, u32[]{:S(2)}, u32[]{:S(2)}) collective-permute-start(bf16[48,2048]{1,0:T(8,128)(2,1)S(1)} %sum_rows.10), channel_id=1, source_target_pairs={{0,8},{4,12},{8,0},{12,4},{16,24},{20,28},{24,16},{28,20},{1,9},{5... | collective-permute-start | bytes 589832 | tf_op jit(solution)/shard_map/ppermute | solution.py:25
  191.2 5.3 %collective-permute-done.35.refs_5_ = bf16[48,2048]{1,0:T(8,128)(2,1)S(1)} collective-permute-done((bf16[48,2048]{1,0:T(8,128)(2,1)S(1)}, bf16[48,2048]{1,0:T(8,128)(2,1)S(1)}, u32[]{:S(2)}, u32[]{:S(2)}) %collective-permute-start.35) | collective-permute-done | bytes 196640 | tf_op jit(solution)/shard_map/ppermute | solution.py:25
  202.3 2.6 %blend_rows.1 = bf16[128,2048]{1,0:T(8,128)(2,1)} custom-call(bf16[128,2048]{1,0:T(8,128)(2,1)S(1)} %copy-done.6, bf16[256,384]{1,0:T(8,128)(2,1)S(1)} %mix_weights.1.mix, bf16[48,2048]{1,0:T(8,128)(2,1)S(1)} %sum_rows.8.refs_0_, bf16[48,2048]{1,0:T(8,128)(2,1)} %collective-permute-done.23.refs_1_, bf16[48,2048]{1,0:T(8,128)(2,1)S(1)} %collective-permute-done.25.refs_2_, ...), custom_call_target="tpu_custom_call" | custom-call | flops 402653184 | bytes 2621440 | tf_op jit(solution)/shard_map/blend_rows/pallas_call | solution.py:397
  (139 shorter events, 57.2 us)
Async XLA Ops:
  0.0 38.5 %collective-permute-start.5 = (bf16[512,2048]{1,0:T(8,128)(2,1)}, bf16[512,2048]{1,0:T(8,128)(2,1)}, u32[]{:S(2)}, u32[]{:S(2)}) collective-permute-start(bf16[512,2048]{1,0:T(8,128)(2,1)} %param.23), channel_id=1, source_target_pairs={{0,1},{1,0},{2,3},{3,2},{4,5},{5,4},{6,7},{7,6},{8,9},{9,8},{10,11... | collective-permute-start | bytes 6291464 | tf_op jit(solution)/shard_map/ppermute | solution.py:29
  32.5 50.6 %collective-permute-start.16 = (bf16[2048,512]{1,0:T(8,128)(2,1)S(1)}, bf16[2048,512]{1,0:T(8,128)(2,1)}, u32[]{:S(2)}, u32[]{:S(2)}) collective-permute-start(bf16[2048,512]{1,0:T(8,128)(2,1)S(1)} %bitcast.33), channel_id=1, source_target_pairs={{0,1},{1,0},{2,3},{3,2},{4,5},{5,4},{6,7},{7,6},{8,9},{9,8},{10,11... | collective-permute-start | bytes 6291464 | tf_op jit(solution)/shard_map/ppermute | solution.py:29
  33.0 50.9 %collective-permute-start.14 = (bf16[2048,512]{1,0:T(8,128)(2,1)}, bf16[2048,512]{1,0:T(8,128)(2,1)}, u32[]{:S(2)}, u32[]{:S(2)}) collective-permute-start(bf16[2048,512]{1,0:T(8,128)(2,1)} %bitcast.37), channel_id=1, source_target_pairs={{0,1},{1,0},{2,3},{3,2},{4,5},{5,4},{6,7},{7,6},{8,9},{9,8},{10,11... | collective-permute-start | bytes 6291464 | tf_op jit(solution)/shard_map/ppermute | solution.py:29
  33.0 61.9 %collective-permute-start.15 = (bf16[2048,512]{1,0:T(8,128)(2,1)}, bf16[2048,512]{1,0:T(8,128)(2,1)}, u32[]{:S(2)}, u32[]{:S(2)}) collective-permute-start(bf16[2048,512]{1,0:T(8,128)(2,1)} %bitcast.41), channel_id=1, source_target_pairs={{0,1},{1,0},{2,3},{3,2},{4,5},{5,4},{6,7},{7,6},{8,9},{9,8},{10,11... | collective-permute-start | bytes 6291464 | tf_op jit(solution)/shard_map/ppermute | solution.py:29
  34.9 15.0 %collective-permute-start.17 = (bf16[512,512]{1,0:T(8,128)(2,1)}, bf16[512,512]{1,0:T(8,128)(2,1)S(1)}, u32[]{:S(2)}, u32[]{:S(2)}) collective-permute-start(bf16[512,512]{1,0:T(8,128)(2,1)} %get-tuple-element.47), channel_id=1, source_target_pairs={{0,2},{1,3},{2,0},{3,1},{4,6},{5,7},{6,4},{7,5},{8,10},{9,11},{10,... | collective-permute-start | bytes 1572872 | tf_op jit(solution)/shard_map/ppermute | solution.py:34
  38.6 22.6 %collective-permute-start.18 = (bf16[512,512]{1,0:T(8,128)(2,1)}, bf16[512,512]{1,0:T(8,128)(2,1)S(1)}, u32[]{:S(2)}, u32[]{:S(2)}) collective-permute-start(bf16[512,512]{1,0:T(8,128)(2,1)} %get-tuple-element.48), channel_id=1, source_target_pairs={{0,2},{1,3},{2,0},{3,1},{4,6},{5,7},{6,4},{7,5},{8,10},{9,11},{10,... | collective-permute-start | bytes 1572872 | tf_op jit(solution)/shard_map/ppermute | solution.py:34
  49.9 21.7 %collective-permute-start.6 = (bf16[128,2048]{1,0:T(8,128)(2,1)}, bf16[128,2048]{1,0:T(8,128)(2,1)}, u32[]{:S(2)}, u32[]{:S(2)}) collective-permute-start(bf16[128,2048]{1,0:T(8,128)(2,1)} %fusion), channel_id=1, source_target_pairs={{0,2},{1,3},{2,0},{3,1},{4,6},{5,7},{6,4},{7,5},{8,10},{9,11},{10,... | collective-permute-start | bytes 1572872 | tf_op jit(solution)/shard_map/ppermute | solution.py:34
  61.1 17.8 %collective-permute-start.19 = (bf16[512,512]{1,0:T(8,128)(2,1)S(1)}, bf16[512,512]{1,0:T(8,128)(2,1)S(1)}, u32[]{:S(2)}, u32[]{:S(2)}) collective-permute-start(bf16[512,512]{1,0:T(8,128)(2,1)S(1)} %collective-permute-done.17.refs_14_.refs_10_), channel_id=1, source_target_pairs={{0,1},{1,0},{2,3},{3,2},{4,5},{5,4},{6,7},{7,6},{8,9},{9,8},{10,11... | collective-permute-start | bytes 1572872 | tf_op jit(solution)/shard_map/ppermute | solution.py:29
  83.1 30.2 %collective-permute-start.28 = (bf16[48,2048]{1,0:T(8,128)(2,1)S(1)}, bf16[48,2048]{1,0:T(8,128)(2,1)S(1)}, u32[]{:S(2)}, u32[]{:S(2)}) collective-permute-start(bf16[48,2048]{1,0:T(8,128)(2,1)S(1)} %get-tuple-element.57), channel_id=1, source_target_pairs={{0,16},{4,20},{8,24},{12,28},{16,0},{20,4},{24,8},{28,12},{1,17},{... | collective-permute-start | bytes 589832 | tf_op jit(solution)/shard_map/ppermute | solution.py:25
  83.9 33.3 %collective-permute-start.29 = (bf16[48,2048]{1,0:T(8,128)(2,1)S(1)}, bf16[48,2048]{1,0:T(8,128)(2,1)S(1)}, u32[]{:S(2)}, u32[]{:S(2)}) collective-permute-start(bf16[48,2048]{1,0:T(8,128)(2,1)S(1)} %get-tuple-element.58), channel_id=1, source_target_pairs={{0,20},{4,16},{8,28},{12,24},{16,4},{20,0},{24,12},{28,8},{1,21},{... | collective-permute-start | bytes 589832 | tf_op jit(solution)/shard_map/ppermute | solution.py:25
  88.7 28.5 %collective-permute-start.38 = (bf16[48,2048]{1,0:T(8,128)(2,1)S(1)}, bf16[48,2048]{1,0:T(8,128)(2,1)S(1)}, u32[]{:S(2)}, u32[]{:S(2)}) collective-permute-start(bf16[48,2048]{1,0:T(8,128)(2,1)S(1)} %collective-permute-done.36.refs_0_), channel_id=1, source_target_pairs={{0,2},{1,3},{2,0},{3,1},{4,6},{5,7},{6,4},{7,5},{8,10},{9,11},{10,... | collective-permute-start | bytes 589832 | tf_op jit(solution)/shard_map/ppermute | solution.py:34
  93.4 25.3 %collective-permute-start.39 = (bf16[48,2048]{1,0:T(8,128)(2,1)S(1)}, bf16[48,2048]{1,0:T(8,128)(2,1)S(1)}, u32[]{:S(2)}, u32[]{:S(2)}) collective-permute-start(bf16[48,2048]{1,0:T(8,128)(2,1)S(1)} %collective-permute-done.37.refs_1_), channel_id=1, source_target_pairs={{0,2},{1,3},{2,0},{3,1},{4,6},{5,7},{6,4},{7,5},{8,10},{9,11},{10,... | collective-permute-start | bytes 589832 | tf_op jit(solution)/shard_map/ppermute | solution.py:34
  94.9 30.0 %collective-permute-start.7 = (bf16[48,2048]{1,0:T(8,128)(2,1)S(1)}, bf16[48,2048]{1,0:T(8,128)(2,1)S(1)}, u32[]{:S(2)}, u32[]{:S(2)}) collective-permute-start(bf16[48,2048]{1,0:T(8,128)(2,1)S(1)} %get-tuple-element.44), channel_id=1, source_target_pairs={{0,4},{4,0},{8,12},{12,8},{16,20},{20,16},{24,28},{28,24},{1,5},{5... | collective-permute-start | bytes 589832 | tf_op jit(solution)/shard_map/ppermute | solution.py:25
  113.3 13.2 %collective-permute-start.8 = (bf16[48,2048]{1,0:T(8,128)(2,1)S(1)}, bf16[48,2048]{1,0:T(8,128)(2,1)S(1)}, u32[]{:S(2)}, u32[]{:S(2)}) collective-permute-start(bf16[48,2048]{1,0:T(8,128)(2,1)S(1)} %get-tuple-element.45), channel_id=1, source_target_pairs={{0,8},{4,12},{8,0},{12,4},{16,24},{20,28},{24,16},{28,20},{1,9},{5... | collective-permute-start | bytes 589832 | tf_op jit(solution)/shard_map/ppermute | solution.py:25
  117.2 11.4 %collective-permute-start.30 = (bf16[48,2048]{1,0:T(8,128)(2,1)S(1)}, bf16[48,2048]{1,0:T(8,128)(2,1)S(1)}, u32[]{:S(2)}, u32[]{:S(2)}) collective-permute-start(bf16[48,2048]{1,0:T(8,128)(2,1)S(1)} %collective-permute-done.28.refs_0_), channel_id=1, source_target_pairs={{0,2},{1,3},{2,0},{3,1},{4,6},{5,7},{6,4},{7,5},{8,10},{9,11},{10,... | collective-permute-start | bytes 589832 | tf_op jit(solution)/shard_map/ppermute | solution.py:34
  127.1 14.5 %collective-permute-start.12 = (bf16[48,2048]{1,0:T(8,128)(2,1)S(1)}, bf16[48,2048]{1,0:T(8,128)(2,1)S(1)}, u32[]{:S(2)}, u32[]{:S(2)}) collective-permute-start(bf16[48,2048]{1,0:T(8,128)(2,1)S(1)} %collective-permute-done.8.refs_2_), channel_id=1, source_target_pairs={{0,2},{1,3},{2,0},{3,1},{4,6},{5,7},{6,4},{7,5},{8,10},{9,11},{10,... | collective-permute-start | bytes 589832 | tf_op jit(solution)/shard_map/ppermute | solution.py:34
  128.6 17.2 %collective-permute-start.13 = (bf16[48,2048]{1,0:T(8,128)(2,1)S(1)}, bf16[48,2048]{1,0:T(8,128)(2,1)S(1)}, u32[]{:S(2)}, u32[]{:S(2)}) collective-permute-start(bf16[48,2048]{1,0:T(8,128)(2,1)S(1)} %collective-permute-done.9.refs_3_), channel_id=1, source_target_pairs={{0,2},{1,3},{2,0},{3,1},{4,6},{5,7},{6,4},{7,5},{8,10},{9,11},{10,... | collective-permute-start | bytes 589832 | tf_op jit(solution)/shard_map/ppermute | solution.py:34
  129.1 26.4 %collective-permute-start.42 = (bf16[48,2048]{1,0:T(8,128)(2,1)S(1)}, bf16[48,2048]{1,0:T(8,128)(2,1)S(1)}, u32[]{:S(2)}, u32[]{:S(2)}) collective-permute-start(bf16[48,2048]{1,0:T(8,128)(2,1)S(1)} %get-tuple-element.68), channel_id=1, source_target_pairs={{0,2},{1,3},{2,0},{3,1},{4,6},{5,7},{6,4},{7,5},{8,10},{9,11},{10,... | collective-permute-start | bytes 589832 | tf_op jit(solution)/shard_map/ppermute | solution.py:34
  136.3 19.8 %collective-permute-start.40 = (bf16[48,2048]{1,0:T(8,128)(2,1)S(1)}, bf16[48,2048]{1,0:T(8,128)(2,1)S(1)}, u32[]{:S(2)}, u32[]{:S(2)}) collective-permute-start(bf16[48,2048]{1,0:T(8,128)(2,1)S(1)} %get-tuple-element.66), channel_id=1, source_target_pairs={{0,2},{1,3},{2,0},{3,1},{4,6},{5,7},{6,4},{7,5},{8,10},{9,11},{10,... | collective-permute-start | bytes 589832 | tf_op jit(solution)/shard_map/ppermute | solution.py:34
  137.4 21.1 %collective-permute-start.34 = (bf16[48,2048]{1,0:T(8,128)(2,1)S(1)}, bf16[48,2048]{1,0:T(8,128)(2,1)S(1)}, u32[]{:S(2)}, u32[]{:S(2)}) collective-permute-start(bf16[48,2048]{1,0:T(8,128)(2,1)S(1)} %get-tuple-element.62), channel_id=1, source_target_pairs={{0,2},{1,3},{2,0},{3,1},{4,6},{5,7},{6,4},{7,5},{8,10},{9,11},{10,... | collective-permute-start | bytes 589832 | tf_op jit(solution)/shard_map/ppermute | solution.py:34
  141.6 21.1 %collective-permute-start.32 = (bf16[48,2048]{1,0:T(8,128)(2,1)S(1)}, bf16[48,2048]{1,0:T(8,128)(2,1)S(1)}, u32[]{:S(2)}, u32[]{:S(2)}) collective-permute-start(bf16[48,2048]{1,0:T(8,128)(2,1)S(1)} %get-tuple-element.60), channel_id=1, source_target_pairs={{0,2},{1,3},{2,0},{3,1},{4,6},{5,7},{6,4},{7,5},{8,10},{9,11},{10,... | collective-permute-start | bytes 589832 | tf_op jit(solution)/shard_map/ppermute | solution.py:34
  153.9 12.9 %collective-permute-start.26 = (bf16[48,2048]{1,0:T(8,128)(2,1)S(1)}, bf16[48,2048]{1,0:T(8,128)(2,1)S(1)}, u32[]{:S(2)}, u32[]{:S(2)}) collective-permute-start(bf16[48,2048]{1,0:T(8,128)(2,1)S(1)} %get-tuple-element.56), channel_id=1, source_target_pairs={{0,2},{1,3},{2,0},{3,1},{4,6},{5,7},{6,4},{7,5},{8,10},{9,11},{10,... | collective-permute-start | bytes 589832 | tf_op jit(solution)/shard_map/ppermute | solution.py:34
  155.5 15.5 %collective-permute-start.24 = (bf16[48,2048]{1,0:T(8,128)(2,1)S(1)}, bf16[48,2048]{1,0:T(8,128)(2,1)S(1)}, u32[]{:S(2)}, u32[]{:S(2)}) collective-permute-start(bf16[48,2048]{1,0:T(8,128)(2,1)S(1)} %get-tuple-element.54), channel_id=1, source_target_pairs={{0,2},{1,3},{2,0},{3,1},{4,6},{5,7},{6,4},{7,5},{8,10},{9,11},{10,... | collective-permute-start | bytes 589832 | tf_op jit(solution)/shard_map/ppermute | solution.py:34
  156.1 19.2 %collective-permute-start.22 = (bf16[48,2048]{1,0:T(8,128)(2,1)S(1)}, bf16[48,2048]{1,0:T(8,128)(2,1)S(1)}, u32[]{:S(2)}, u32[]{:S(2)}) collective-permute-start(bf16[48,2048]{1,0:T(8,128)(2,1)S(1)} %get-tuple-element.52), channel_id=1, source_target_pairs={{0,2},{1,3},{2,0},{3,1},{4,6},{5,7},{6,4},{7,5},{8,10},{9,11},{10,... | collective-permute-start | bytes 589832 | tf_op jit(solution)/shard_map/ppermute | solution.py:34
  158.4 20.5 %collective-permute-start.21 = (bf16[48,2048]{1,0:T(8,128)(2,1)S(1)}, bf16[48,2048]{1,0:T(8,128)(2,1)S(1)}, u32[]{:S(2)}, u32[]{:S(2)}) collective-permute-start(bf16[48,2048]{1,0:T(8,128)(2,1)S(1)} %get-tuple-element.50), channel_id=1, source_target_pairs={{0,2},{1,3},{2,0},{3,1},{4,6},{5,7},{6,4},{7,5},{8,10},{9,11},{10,... | collective-permute-start | bytes 589832 | tf_op jit(solution)/shard_map/ppermute | solution.py:34
  162.6 18.3 %collective-permute-start.43 = (bf16[48,2048]{1,0:T(8,128)(2,1)S(1)}, bf16[48,2048]{1,0:T(8,128)(2,1)S(1)}, u32[]{:S(2)}, u32[]{:S(2)}) collective-permute-start(bf16[48,2048]{1,0:T(8,128)(2,1)S(1)} %sum_rows.15), channel_id=1, source_target_pairs={{0,28},{4,24},{8,20},{12,16},{16,12},{20,8},{24,4},{28,0},{1,29},{... | collective-permute-start | bytes 589832 | tf_op jit(solution)/shard_map/ppermute | solution.py:25
  166.9 22.2 %collective-permute-start.41 = (bf16[48,2048]{1,0:T(8,128)(2,1)S(1)}, bf16[48,2048]{1,0:T(8,128)(2,1)S(1)}, u32[]{:S(2)}, u32[]{:S(2)}) collective-permute-start(bf16[48,2048]{1,0:T(8,128)(2,1)S(1)} %sum_rows.14), channel_id=1, source_target_pairs={{0,24},{4,28},{8,16},{12,20},{16,8},{20,12},{24,0},{28,4},{1,25},{... | collective-permute-start | bytes 589832 | tf_op jit(solution)/shard_map/ppermute | solution.py:25
  171.1 25.4 %collective-permute-start.35 = (bf16[48,2048]{1,0:T(8,128)(2,1)S(1)}, bf16[48,2048]{1,0:T(8,128)(2,1)S(1)}, u32[]{:S(2)}, u32[]{:S(2)}) collective-permute-start(bf16[48,2048]{1,0:T(8,128)(2,1)S(1)} %sum_rows.13), channel_id=1, source_target_pairs={{0,20},{4,16},{8,28},{12,24},{16,4},{20,0},{24,12},{28,8},{1,21},{... | collective-permute-start | bytes 589832 | tf_op jit(solution)/shard_map/ppermute | solution.py:25
  175.3 23.7 %collective-permute-start.33 = (bf16[48,2048]{1,0:T(8,128)(2,1)S(1)}, bf16[48,2048]{1,0:T(8,128)(2,1)}, u32[]{:S(2)}, u32[]{:S(2)}) collective-permute-start(bf16[48,2048]{1,0:T(8,128)(2,1)S(1)} %sum_rows.12), channel_id=1, source_target_pairs={{0,16},{4,20},{8,24},{12,28},{16,0},{20,4},{24,8},{28,12},{1,17},{... | collective-permute-start | bytes 589832 | tf_op jit(solution)/shard_map/ppermute | solution.py:25
  179.0 20.0 %collective-permute-start.27 = (bf16[48,2048]{1,0:T(8,128)(2,1)S(1)}, bf16[48,2048]{1,0:T(8,128)(2,1)}, u32[]{:S(2)}, u32[]{:S(2)}) collective-permute-start(bf16[48,2048]{1,0:T(8,128)(2,1)S(1)} %sum_rows.11), channel_id=1, source_target_pairs={{0,12},{4,8},{8,4},{12,0},{16,28},{20,24},{24,20},{28,16},{1,13},{... | collective-permute-start | bytes 589832 | tf_op jit(solution)/shard_map/ppermute | solution.py:25
  181.0 19.5 %collective-permute-start.25 = (bf16[48,2048]{1,0:T(8,128)(2,1)S(1)}, bf16[48,2048]{1,0:T(8,128)(2,1)S(1)}, u32[]{:S(2)}, u32[]{:S(2)}) collective-permute-start(bf16[48,2048]{1,0:T(8,128)(2,1)S(1)} %sum_rows.10), channel_id=1, source_target_pairs={{0,8},{4,12},{8,0},{12,4},{16,24},{20,28},{24,16},{28,20},{1,9},{5... | collective-permute-start | bytes 589832 | tf_op jit(solution)/shard_map/ppermute | solution.py:25
  189.0 11.4 %collective-permute-start.23 = (bf16[48,2048]{1,0:T(8,128)(2,1)S(1)}, bf16[48,2048]{1,0:T(8,128)(2,1)}, u32[]{:S(2)}, u32[]{:S(2)}) collective-permute-start(bf16[48,2048]{1,0:T(8,128)(2,1)S(1)} %sum_rows.9), channel_id=1, source_target_pairs={{0,4},{4,0},{8,12},{12,8},{16,20},{20,16},{24,28},{28,24},{1,5},{5... | collective-permute-start | bytes 589832 | tf_op jit(solution)/shard_map/ppermute | solution.py:25
  (33 other events, 440.3 us)
